TPU v7x, 32 devices: a whole 2x2x4 slice. The times are simulated.
32 devices in a mesh: grp: 2 (over y), sp: 4 (over z), tp: 4 (over x, core).
Axes of the slice: x: 2, y: 2, z: 4, core: 2. Of those that a mesh axis runs over, the one named last changes fastest.
Arguments:
- prompt: bfloat16 [8, 6144, 2048], P('grp', 'sp'), parts along dimension 0, may hold values from -6 to 6
- w_key: bfloat16 [2048, 2048], P('sp', 'tp'), may hold values from -0.125 to 0.125
- w_value: bfloat16 [2048, 2048], P('sp', 'tp'), may hold values from -0.125 to 0.125
- query_new: bfloat16 [8, 2048], P('grp', 'tp'), parts along dimension 0, may hold values from -150 to 150
- key_new: bfloat16 [8, 2048], P('grp', 'tp'), parts along dimension 0, may hold values from -15 to 15
- value_new: bfloat16 [8, 2048], P('grp', 'tp'), parts along dimension 0, may hold values from -6 to 6
- mix_lambda: float32 [16], P('tp'), may hold values from 0.3 to 0.8
- head_gain: float32 [128], replicated, may hold values from 0.1 to 1.9
Outputs:
- key_cache: bfloat16 [8, 4, 1536, 2048], P(('grp', 'sp'), None, None, 'tp'), parts along dimension 0
- value_cache: bfloat16 [8, 4, 1536, 2048], P(('grp', 'sp'), None, None, 'tp'), parts along dimension 0
- first_read: bfloat16 [8, 2048], P('grp', 'tp'), parts along dimension 0
There are 2 independent parts, one for each index of `grp`. A program takes and returns all parts, laid end to end along the dimension named above; an argument that names none is the same for every part. Nothing has to cross between parts.
All inputs are finite; a program needn't handle non-finite values.
Results may differ from a plain program's by a relative error of at most 0.0065.
The roundings to bfloat16 on the way count: a program that leaves them out, or rounds other values in their place, can miss the bound.
Values may be sent and summed in bfloat16 or wider, within the bound.
A program may use at most 128 MiB of HBM per device.

v0:
```python
import functools

import jax
import jax.numpy as jnp
from jax import lax
from jax.experimental import pallas as pl
from jax.experimental.pallas import tpu as pltpu
from jax.sharding import PartitionSpec as P

HALF = 64
VDIM = 128
MESH = pl.DeviceIdType.MESH
CHUNKS = 8
LAG_X = 1
LAG_C = 2
EARLY = 2
AHEAD = 24


def combined_all(part, axis, combine):
    gathered = jax.tree.map(lambda a: lax.all_gather(a, axis), part)

    def take(source):
        return jax.tree.map(lambda a: lax.dynamic_index_in_dim(a, source, 0, False), gathered)

    return lax.fori_loop(
        1, lax.axis_size(axis), lambda source, state: combine(state, take(source)), take(0)
    )


def project(rows, w_key, w_value):
    keys = jnp.dot(
        rows, lax.all_gather(w_key, "sp", axis=0, tiled=True), preferred_element_type=jnp.float32
    )
    values = jnp.dot(
        rows, lax.all_gather(w_value, "sp", axis=0, tiled=True), preferred_element_type=jnp.float32
    )
    return (keys.astype(jnp.bfloat16), values.astype(jnp.bfloat16))


def score_maps(query, keys):
    count, span = (keys.shape[0], keys.shape[1])
    heads = query.shape[1] // (2 * HALF)
    q_parts = query.reshape(count, heads, 2, HALF)
    k_parts = keys.reshape(count, span, heads, 2, HALF)
    return jnp.einsum(
        "shmc,slhmc->shml", q_parts, k_parts, preferred_element_type=jnp.float32
    ) * HALF ** (-0.5)


def own_scores(query, fresh_key):
    count = query.shape[0]
    heads = query.shape[1] // (2 * HALF)
    q_parts = query.astype(jnp.float32).reshape(count, heads, 2, HALF)
    k_parts = fresh_key.astype(jnp.float32).reshape(count, heads, 2, HALF)
    return jnp.sum(q_parts * k_parts, axis=-1) * HALF ** (-0.5)


def finish(reads, head_gain):
    mean = jnp.mean(reads * reads, axis=-1, keepdims=True)
    normed = reads * lax.rsqrt(mean + 1e-06) * head_gain
    return normed.reshape(reads.shape[0], -1).astype(jnp.bfloat16)


def join_totals(first, second):
    top = jnp.maximum(first[0], second[0])
    return (top, first[1] * jnp.exp(first[0] - top) + second[1] * jnp.exp(second[0] - top))


def placed(part_rows, prompts, first, fill):
    base = jnp.full((prompts,) + part_rows.shape[1:], fill, jnp.float32)
    return lax.dynamic_update_slice_in_dim(base, part_rows, first, 0)


def cache_read(query_new, key_new, value_new, keys, values, mix_lambda, head_gain, first):
    count, span = (keys.shape[0], keys.shape[1])
    prompts = query_new.shape[0]
    heads = mix_lambda.shape[0]
    query = lax.dynamic_slice_in_dim(query_new, first, count, 0)
    scores = score_maps(query, keys)
    fresh_all = own_scores(query_new, key_new)
    fresh = lax.dynamic_slice_in_dim(fresh_all, first, count, 0)
    local_top = jnp.maximum(jnp.max(scores, axis=-1), fresh)
    local_total = jnp.sum(jnp.exp(scores - local_top[..., None]), axis=-1)
    top_all, cache_total = combined_all(
        (placed(local_top, prompts, first, -1e30), placed(local_total, prompts, first, 0.0)),
        "sp",
        join_totals,
    )
    own = jnp.exp(fresh_all - top_all)
    total_all = cache_total + own
    top = lax.dynamic_slice_in_dim(top_all, first, count, 0)
    total = lax.dynamic_slice_in_dim(total_all, first, count, 0)
    probs = jnp.exp(scores - top[..., None]) / total[..., None]
    mixed = (probs[:, :, 0] - mix_lambda[None, :, None] * probs[:, :, 1]).astype(jnp.bfloat16)
    value_parts = values.reshape(count, span, heads, VDIM)
    partial_value = jnp.einsum(
        "shl,slhv->shv", mixed, value_parts, preferred_element_type=jnp.float32
    )
    reads = lax.psum(placed(partial_value, prompts, first, 0.0), "sp")
    own_prob = own / total_all
    own_mixed = (own_prob[:, :, 0] - mix_lambda[None, :] * own_prob[:, :, 1]).astype(jnp.bfloat16)
    reads = reads + own_mixed.astype(jnp.float32)[..., None] * value_new.astype(
        jnp.float32
    ).reshape(prompts, heads, VDIM)
    return finish(reads, head_gain)


def block_read(
    query_new, key_new, value_new, key_cache, value_cache, mix_lambda, head_gain, spread
):
    blocks, sub = (key_cache.shape[1], key_cache.shape[2])
    first = lax.axis_index("sp") // spread
    keys = key_cache.reshape(1, blocks * sub, -1)
    values = value_cache.reshape(1, blocks * sub, -1)
    return cache_read(query_new, key_new, value_new, keys, values, mix_lambda, head_gain, first)


def body(prompt, w_key, w_value, query_new, key_new, value_new, mix_lambda, head_gain):
    count, piece, width = prompt.shape
    spread = lax.axis_size("sp") // count
    sub = piece // spread
    keys, values = project(prompt.reshape(count * piece, width), w_key, w_value)
    key_blocks = keys.reshape(count * spread, 1, sub, -1)
    value_blocks = values.reshape(count * spread, 1, sub, -1)
    key_cache, value_cache = (
        lax.all_to_all(key_blocks, "sp", split_axis=0, concat_axis=1, tiled=True),
        lax.all_to_all(value_blocks, "sp", split_axis=0, concat_axis=1, tiled=True),
    )
    first_read = block_read(
        query_new, key_new, value_new, key_cache, value_cache, mix_lambda, head_gain, spread
    )
    return (key_cache, value_cache, first_read)


def gather_kernel(
    sizes, prompt, w_key, w_value, keys, values,
    rows_in, weights,
    z_send, z_recv, x_send, x_recv, d_send, d_recv, e_send, e_recv,
    wr_send, wr_recv, wl_send, wl_recv, wy_send, wy_recv, local,
):
    n, chunks, tile, quarter = sizes
    me = lax.axis_index("sp")
    tp = lax.axis_index("tp")
    grp = lax.axis_index("grp")
    across = lax.rem(tp + 2, 4)
    sibling = tp + 1 - 2 * lax.rem(tp, 2)
    far = lax.rem(sibling + 2, 4)
    depth, cols = w_key.shape
    half = depth // 2
    mats = (w_key, w_value)

    def rows(j, q):
        return pl.ds(pl.multiple_of(j * tile + q * quarter, quarter), quarter)

    barrier = pltpu.get_barrier_semaphore()
    for step in range(1, n):
        pl.semaphore_signal(
            barrier, inc=1, device_id={"sp": lax.rem(me + step, n)}, device_id_type=MESH
        )
    pl.semaphore_signal(barrier, inc=1, device_id={"tp": across}, device_id_type=MESH)
    pl.semaphore_signal(barrier, inc=1, device_id={"tp": sibling}, device_id_type=MESH)
    pl.semaphore_signal(barrier, inc=1, device_id={"grp": 1 - grp}, device_id_type=MESH)
    pl.semaphore_wait(barrier, n + 2)

    def w_slot(src, m, g):
        return weights.at[pl.ds(pl.multiple_of(src * depth + g * half, half), half),
                          pl.ds(m * cols, cols)]

    def w_hop(src, m, to, send, recv, own):
        origin = mats[m].at[pl.ds(pl.multiple_of(grp * half, half), half)] if own else w_slot(src, m, grp)
        return pltpu.make_async_remote_copy(
            src_ref=origin, dst_ref=w_slot(src, m, grp),
            send_sem=send.at[src * 2 + m], recv_sem=recv.at[src * 2 + m],
            device_id={"sp": to}, device_id_type=MESH,
        )

    def w_side(src, m, g):
        return pltpu.make_async_remote_copy(
            src_ref=w_slot(src, m, g), dst_ref=w_slot(src, m, g),
            send_sem=wy_send.at[src * 2 + m], recv_sem=wy_recv.at[src * 2 + m],
            device_id={"grp": 1 - grp}, device_id_type=MESH,
        )

    def z_copy(src, dst, j):
        return pltpu.make_async_remote_copy(
            src_ref=prompt.at[dst, rows(j, tp)], dst_ref=rows_in.at[src, rows(j, tp)],
            send_sem=z_send.at[dst * chunks + j], recv_sem=z_recv.at[src * chunks + j],
            device_id={"sp": dst}, device_id_type=MESH,
        )

    def side_copy(src, j, q, to, send, recv):
        return pltpu.make_async_remote_copy(
            src_ref=rows_in.at[src, rows(j, q)], dst_ref=rows_in.at[src, rows(j, q)],
            send_sem=send.at[src * chunks + j], recv_sem=recv.at[src * chunks + j],
            device_id={"tp": to}, device_id_type=MESH,
        )

    def right_send(i):
        @pl.when(i < (n - 1 - me) * chunks)
        def _():
            c = jnp.maximum(n - 1 - me, 1)
            z_copy(me, me + c - lax.rem(i, c), i // c).start()

    def left_send(i):
        @pl.when(i < me * chunks)
        def _():
            c = jnp.maximum(me, 1)
            z_copy(me, me - c + lax.rem(i, c), i // c).start()

    def both_sends(i, carry):
        right_send(i)
        left_send(i)
        return carry

    for m in range(2):
        @pl.when(me + 1 < n)
        def _():
            w_hop(me, m, me + 1, wr_send, wr_recv, True).start()

        @pl.when(me > 0)
        def _():
            w_hop(me, m, me - 1, wl_send, wl_recv, True).start()

    own_w = [
        pltpu.make_async_copy(
            mats[m],
            weights.at[pl.ds(pl.multiple_of(me * depth, depth), depth), pl.ds(m * cols, cols)],
            local.at[m],
        )
        for m in range(2)
    ]
    own_rows = pltpu.make_async_copy(prompt.at[me], rows_in.at[me], local.at[2])
    for copy in own_w:
        copy.start()
    own_rows.start()

    @pl.when(me == 0)
    def _():
        for i in range(EARLY):
            right_send(i)

    @pl.when(me == n - 1)
    def _():
        for i in range(EARLY):
            left_send(i)

    for d in range(1, n):
        @pl.when(me - d >= 0)
        def _():
            for m in range(2):
                w_hop(me - d, m, me, wr_send, wr_recv, False).wait_recv()

                @pl.when(me + 1 < n)
                def _():
                    w_hop(me - d, m, me + 1, wr_send, wr_recv, False).start()

                w_side(me - d, m, grp).start()

        @pl.when(me + d < n)
        def _():
            for m in range(2):
                w_hop(me + d, m, me, wl_send, wl_recv, False).wait_recv()

                @pl.when(me > 0)
                def _():
                    w_hop(me + d, m, me - 1, wl_send, wl_recv, False).start()

                w_side(me + d, m, grp).start()

        @pl.when(me == d)
        def _():
            for i in range(EARLY):
                right_send(i)

        @pl.when(n - 1 - me == d)
        def _():
            for i in range(EARLY):
                left_send(i)

    lax.fori_loop(EARLY, AHEAD, both_sends, 0)

    for step in range(1, n):
        src = lax.rem(me + step, n)
        for m in range(2):
            w_side(src, m, 1 - grp).wait_recv()
    for copy in own_w:
        copy.wait()
    own_rows.wait()

    def compute(src, j):
        where = pl.ds(pl.multiple_of(j * tile, tile), tile)
        both = jnp.dot(
            rows_in[src, where, :], weights[...], preferred_element_type=jnp.float32
        ).astype(jnp.bfloat16)
        keys[src, where, :] = both[:, :cols]
        values[src, where, :] = both[:, cols:]

    def order(k):
        pick = k * 0
        for spot in range(n):
            seq = []
            for j in range(chunks):
                for src in sorted(range(n), key=lambda a: -abs(a - spot)):
                    if src != spot:
                        slow = (src in (n // 2 - 1, n // 2)) and ((src < n // 2) != (spot < n // 2))
                        seq.append((j * 2 + (3 if slow else 0), len(seq), src * chunks + j))
            for at, (_, _, value) in enumerate(sorted(seq)):
                pick = jnp.where((me == spot) & (k == at), value, pick)
        return pick // chunks, lax.rem(pick, chunks)

    total = (n - 1) * chunks

    def step(k, carry):
        both_sends(AHEAD + k, 0)

        @pl.when(k < total)
        def _():
            src, j = order(k)
            z_copy(src, me, j).wait_recv()
            side_copy(src, j, tp, across, x_send, x_recv).start()
            side_copy(src, j, tp, sibling, d_send, d_recv).start()

        @pl.when((k >= LAG_X) & (k < total + LAG_X))
        def _():
            src, j = order(k - LAG_X)
            side_copy(src, j, across, across, x_send, x_recv).wait_recv()
            side_copy(src, j, across, sibling, e_send, e_recv).start()

        @pl.when(k < chunks)
        def _():
            compute(me, k)

        @pl.when(k >= LAG_C)
        def _():
            src, j = order(k - LAG_C)
            side_copy(src, j, sibling, sibling, d_send, d_recv).wait_recv()
            side_copy(src, j, far, sibling, e_send, e_recv).wait_recv()
            compute(src, j)

        return carry

    lax.fori_loop(0, total + LAG_C, step, 0)

    def drain(k, carry):
        src, j = order(k)
        z_copy(me, src, j).wait_send()
        side_copy(src, j, tp, across, x_send, x_recv).wait_send()
        side_copy(src, j, tp, sibling, d_send, d_recv).wait_send()
        side_copy(src, j, across, sibling, e_send, e_recv).wait_send()
        return carry

    lax.fori_loop(0, total, drain, 0)
    for step_ in range(1, n):
        src = lax.rem(me + step_, n)
        for m in range(2):
            w_side(src, m, grp).wait_send()
    for d in range(n):
        for m in range(2):
            @pl.when((me - d >= 0) & (me + 1 < n))
            def _():
                w_hop(me - d, m, me + 1, wr_send, wr_recv, False).wait_send()

            @pl.when((me + d < n) & (me > 0))
            def _():
                w_hop(me + d, m, me - 1, wl_send, wl_recv, False).wait_send()


def gather_project(n, prompt, w_key, w_value):
    count, piece, width = prompt.shape
    depth, cols = w_key.shape
    tile = piece // CHUNKS
    quarter = tile // 4
    dma = pltpu.SemaphoreType.DMA
    steps = n * CHUNKS
    out = pltpu.VMEM((n, piece, cols), jnp.bfloat16)
    vmem = pl.BlockSpec(memory_space=pltpu.VMEM)
    hbm = pl.BlockSpec(memory_space=pl.ANY)
    return pl.pallas_call(
        functools.partial(gather_kernel, (n, CHUNKS, tile, quarter)),
        out_shape=(out, out),
        in_specs=[hbm] * 3,
        out_specs=(vmem, vmem),
        scratch_shapes=[
            pltpu.VMEM((n, piece, width), jnp.bfloat16),
            pltpu.VMEM((n * depth, 2 * cols), jnp.bfloat16),
        ]
        + [dma((steps,))] * 8
        + [dma((2 * n,))] * 6
        + [dma((3,))],
        compiler_params=pltpu.CompilerParams(
            collective_id=0, has_side_effects=True, vmem_limit_bytes=36 * 2**20
        ),
    )(prompt, w_key, w_value)


def read_kernel(
    pieces, query, key_new, value_new, lam, gain, k_all, v_all, keys, values, read,
    scores, out_sem,
):
    span, cols = k_all.shape
    tile = span // pieces
    heads = cols // VDIM
    me = lax.axis_index("sp")
    stores = (
        pltpu.make_async_copy(k_all, keys, out_sem.at[0]),
        pltpu.make_async_copy(v_all, values, out_sem.at[1]),
    )
    for copy in stores:
        copy.start()

    def mine(ref):
        whole = ref[...].astype(jnp.float32)
        here = lax.broadcasted_iota(jnp.int32, whole.shape, 0) == me
        return jnp.sum(jnp.where(here, whole, 0.0), axis=0, keepdims=True)

    shape = (2 * heads, cols)
    row = lax.broadcasted_iota(jnp.int32, shape, 0)
    group = lax.broadcasted_iota(jnp.int32, shape, 1) // HALF
    part = jnp.where(row < heads, 2 * row, 2 * (row - heads) + 1) == group
    q_row = mine(query)
    q_mat = jnp.where(part, jnp.broadcast_to(q_row, shape), 0.0)
    scale = HALF ** (-0.5)
    fresh = jnp.sum(q_mat * mine(key_new), axis=1, keepdims=True) * scale
    q_low = q_mat.astype(jnp.bfloat16)
    for i in range(pieces):
        scores[:, i * tile:(i + 1) * tile] = lax.dot_general(
            q_low, k_all[i * tile:(i + 1) * tile, :], (((1,), (1,)), ((), ())),
            preferred_element_type=jnp.float32,
        ) * scale
    s = scores[...]
    top = jnp.maximum(jnp.max(s, axis=1, keepdims=True), fresh)
    e = jnp.exp(s - top)
    own = jnp.exp(fresh - top)
    total = jnp.sum(e, axis=1, keepdims=True) + own
    w = e / total
    own = own / total
    mix = lam[...]
    mixed = (w[:heads] - mix * w[heads:]).astype(jnp.bfloat16)
    own_mixed = (own[:heads] - mix * own[heads:]).astype(jnp.bfloat16).astype(jnp.float32)
    o = jnp.dot(mixed, v_all[...], preferred_element_type=jnp.float32)
    o = o + own_mixed * mine(value_new)
    for h in range(heads):
        lanes = slice(h * VDIM, (h + 1) * VDIM)
        one = o[h:h + 1, lanes]
        mean = jnp.mean(one * one, axis=1, keepdims=True)
        read[:, lanes] = one * lax.rsqrt(mean + 1e-06) * gain[...]
    for copy in stores:
        copy.wait()


def read_call(query, key_new, value_new, mix_lambda, head_gain, keys, values):
    span, cols = keys.shape
    heads = mix_lambda.shape[0]
    pieces = 12
    hbm = pl.BlockSpec(memory_space=pl.ANY)
    vmem = pl.BlockSpec(memory_space=pltpu.VMEM)
    out = jax.ShapeDtypeStruct((span, cols), jnp.bfloat16)
    dma = pltpu.SemaphoreType.DMA
    return pl.pallas_call(
        functools.partial(read_kernel, pieces),
        out_shape=(out, out, jax.ShapeDtypeStruct((1, cols), jnp.float32)),
        in_specs=[vmem] * 7,
        out_specs=(hbm, hbm, vmem),
        scratch_shapes=[
            pltpu.VMEM((2 * heads, span), jnp.float32),
            dma((2,)),
        ],
        compiler_params=pltpu.CompilerParams(vmem_limit_bytes=32 * 2**20),
    )(query, key_new, value_new, mix_lambda[:, None], head_gain[None, :], keys, values)


def share_kernel(n, mine, out, slots, send_sem, recv_sem):
    me = lax.axis_index("sp")
    barrier = pltpu.get_barrier_semaphore()
    for step in range(1, n):
        pl.semaphore_signal(
            barrier, inc=1, device_id={"sp": lax.rem(me + step, n)}, device_id_type=MESH
        )
    pl.semaphore_wait(barrier, n - 1)

    def copy(step, src):
        return pltpu.make_async_remote_copy(
            src_ref=mine, dst_ref=slots.at[src],
            send_sem=send_sem.at[step], recv_sem=recv_sem.at[src],
            device_id={"sp": lax.rem(me + step, n)}, device_id_type=MESH,
        )

    for step in range(1, n):
        copy(step, me).start()
    for step in range(1, n):
        copy(step, lax.rem(me + step, n)).wait_recv()
    row = mine[...]
    for src in range(n):
        out[src:src + 1, :] = jnp.where(me == src, row, slots[src]).astype(jnp.bfloat16)
    for step in range(1, n):
        copy(step, me).wait_send()


def share(n, read):
    vmem = pl.BlockSpec(memory_space=pltpu.VMEM)
    dma = pltpu.SemaphoreType.DMA
    return pl.pallas_call(
        functools.partial(share_kernel, n),
        out_shape=jax.ShapeDtypeStruct((n, read.shape[1]), jnp.bfloat16),
        in_specs=[vmem],
        out_specs=vmem,
        scratch_shapes=[
            pltpu.VMEM((n, 1, read.shape[1]), jnp.float32), dma((n,)), dma((n,)),
        ],
        compiler_params=pltpu.CompilerParams(
            collective_id=1, has_side_effects=True, vmem_limit_bytes=2**20
        ),
    )(read)


def fast_body(prompt, w_key, w_value, query_new, key_new, value_new, mix_lambda, head_gain):
    count, piece, width = prompt.shape
    n = lax.axis_size("sp")
    keys, values = gather_project(n, prompt, w_key, w_value)
    cols = keys.shape[-1]
    keys, values, read = read_call(
        query_new, key_new, value_new, mix_lambda, head_gain,
        keys.reshape(n * piece, cols), values.reshape(n * piece, cols),
    )
    return (
        keys.reshape(1, n, piece, cols),
        values.reshape(1, n, piece, cols),
        share(n, read),
    )


def choose(mesh):
    def run(prompt, *rest):
        sizes = dict(mesh.shape)
        count, piece, width = prompt.shape
        rows = rest[0].shape[0]
        fits = (
            sizes["grp"] == 2
            and sizes["tp"] == 4
            and sizes["sp"] == count
            and count > 1
            and piece % (64 * CHUNKS) == 0
            and rows % 32 == 0
            and (count * piece) % 1536 == 0
            and count * piece * width * 2 <= 2**25
        )
        return (fast_body if fits else body)(prompt, *rest)

    return run


def solution(mesh):
    placed = (
        P("grp", "sp", None),
        P("sp", "tp"),
        P("sp", "tp"),
        P("grp", "tp"),
        P("grp", "tp"),
        P("grp", "tp"),
        P("tp"),
        P(),
    )
    return jax.shard_map(
        choose(mesh),
        mesh=mesh,
        in_specs=placed,
        out_specs=(
            P(("grp", "sp"), None, None, "tp"),
            P(("grp", "sp"), None, None, "tp"),
            P("grp", "tp"),
        ),
        check_vma=False,
    )
```

profile of v0, /device:TPU:0, one launch (start us, length us, event | category | flops | bytes accessed | tf_op | source)
XLA Modules:
  0.0 191.9 jit_solution(7621364451693554776)
XLA Ops:
  0.6 0.7 copy.11.lam
  1.4 0.0 copy-start
  1.4 1.0 copy-done
  2.4 0.0 copy-start.1
  2.4 1.0 copy-done.1
  3.5 0.0 copy-start.2
  3.5 0.0 copy-start.3
  3.5 0.0 copy-start.4
  3.5 0.0 copy-start.5
  3.5 174.8 %shard_map.103 = (bf16[4,1536,512]{2,1,0:T(8,128)(2,1)S(1)}, bf16[4,1536,512]{2,1,0:T(8,128)(2,1)S(1)}) custom-call(bf16[4,1536,2048]{2,1,0:T(8,128)(2,1)} %prompt.1, bf16[512,512]{1,0:T(8,128)(2,1)S(1)} %copy-done, bf16[512,512]{1,0:T(8,128)(2,1)S(1)} %copy-done.1), custom_call_target="tpu_custom_call" | custom-call | tf_op jit(solution)/shard_map/pallas_call | solution.py:379
  178.3 0.0 copy-done.2
  178.3 0.0 copy-done.3
  178.3 0.0 copy-done.4
  178.3 0.0 copy-done.5
  178.3 4.8 %shard_map.104 = (bf16[6144,512]{1,0:T(8,128)(2,1)}, bf16[6144,512]{1,0:T(8,128)(2,1)}, f32[1,512]{1,0:T(1,128)S(1)}) custom-call(bf16[4,512]{1,0:T(4,128)(2,1)S(1)} %copy-done.2, bf16[4,512]{1,0:T(4,128)(2,1)S(1)} %copy-done.3, bf16[4,512]{1,0:T(4,128)(2,1)S(1)} %copy-done.4, f32[4,1]{1,0:T(4,128)S(1)} %copy.11.lam, f32[1,128]{1,0:T(1,128)S(1)} %bitcast.8, ...), custom_call_target="tpu_custom_call" | custom-call | tf_op jit(solution)/shard_map/pallas_call | solution.py:460
  183.1 8.2 %shard_map.105 = bf16[4,512]{1,0:T(4,128)(2,1)S(1)} custom-call(f32[1,512]{1,0:T(1,128)S(1)} %get-tuple-element.12.mine), custom_call_target="tpu_custom_call" | custom-call | tf_op jit(solution)/shard_map/pallas_call | solution.py:503
  191.3 0.6 copy.13
Async XLA Ops:
  1.4 1.0 copy-start
  2.4 1.0 copy-start.1
  3.5 174.8 %copy-start.2 = (bf16[4,512]{1,0:T(4,128)(2,1)S(1)}, bf16[4,512]{1,0:T(4,128)(2,1)}, u32[]{:S(2)}) copy-start(bf16[4,512]{1,0:T(4,128)(2,1)} %query.1) | copy-start | bytes 12292
  3.5 174.9 %copy-start.3 = (bf16[4,512]{1,0:T(4,128)(2,1)S(1)}, bf16[4,512]{1,0:T(4,128)(2,1)}, u32[]{:S(2)}) copy-start(bf16[4,512]{1,0:T(4,128)(2,1)} %key_new.1) | copy-start | bytes 12292
  3.5 174.9 %copy-start.4 = (bf16[4,512]{1,0:T(4,128)(2,1)S(1)}, bf16[4,512]{1,0:T(4,128)(2,1)}, u32[]{:S(2)}) copy-start(bf16[4,512]{1,0:T(4,128)(2,1)} %value_new.1) | copy-start | bytes 12292
  3.5 174.9 %copy-start.5 = (f32[128]{0:T(128)S(1)}, f32[128]{0:T(128)}, u32[]{:S(2)}) copy-start(f32[128]{0:T(128)} %param.15) | copy-start | bytes 1540
where the time goes:
time: 192 us
  Pallas kernels  188 us (98%)
  local copies, waits for them, and re-layouts  3.43 us (2%)
    pallas_call x1, Pallas kernels, gather_project(): pl.pallas_call(functools.partial(gather_kernel, (n, CHUNKS, tile, quarter...  175 us
    pallas_call x1, Pallas kernels, share(): pl.pallas_call(functools.partial(share_kernel, n), out_shape=jax.ShapeDty...  8.18 us
    pallas_call x1, Pallas kernels, read_call(): pl.pallas_call(functools.partial(read_kernel, pieces), out_shape=(out, ou...  4.8 us

commit v1 on v0

v1 whole, which is shorter than its diff:
```python
import functools

import jax
import jax.numpy as jnp
from jax import lax
from jax.experimental import pallas as pl
from jax.experimental.pallas import tpu as pltpu
from jax.sharding import PartitionSpec as P

HALF = 64
VDIM = 128
MESH = pl.DeviceIdType.MESH
BIG = 256
FILL = 128
SMALL = 64


def combined_all(part, axis, combine):
    gathered = jax.tree.map(lambda a: lax.all_gather(a, axis), part)

    def take(source):
        return jax.tree.map(lambda a: lax.dynamic_index_in_dim(a, source, 0, False), gathered)

    return lax.fori_loop(
        1, lax.axis_size(axis), lambda source, state: combine(state, take(source)), take(0)
    )


def project(rows, w_key, w_value):
    keys = jnp.dot(
        rows, lax.all_gather(w_key, "sp", axis=0, tiled=True), preferred_element_type=jnp.float32
    )
    values = jnp.dot(
        rows, lax.all_gather(w_value, "sp", axis=0, tiled=True), preferred_element_type=jnp.float32
    )
    return (keys.astype(jnp.bfloat16), values.astype(jnp.bfloat16))


def score_maps(query, keys):
    count, span = (keys.shape[0], keys.shape[1])
    heads = query.shape[1] // (2 * HALF)
    q_parts = query.reshape(count, heads, 2, HALF)
    k_parts = keys.reshape(count, span, heads, 2, HALF)
    return jnp.einsum(
        "shmc,slhmc->shml", q_parts, k_parts, preferred_element_type=jnp.float32
    ) * HALF ** (-0.5)


def own_scores(query, fresh_key):
    count = query.shape[0]
    heads = query.shape[1] // (2 * HALF)
    q_parts = query.astype(jnp.float32).reshape(count, heads, 2, HALF)
    k_parts = fresh_key.astype(jnp.float32).reshape(count, heads, 2, HALF)
    return jnp.sum(q_parts * k_parts, axis=-1) * HALF ** (-0.5)


def finish(reads, head_gain):
    mean = jnp.mean(reads * reads, axis=-1, keepdims=True)
    normed = reads * lax.rsqrt(mean + 1e-06) * head_gain
    return normed.reshape(reads.shape[0], -1).astype(jnp.bfloat16)


def join_totals(first, second):
    top = jnp.maximum(first[0], second[0])
    return (top, first[1] * jnp.exp(first[0] - top) + second[1] * jnp.exp(second[0] - top))


def placed(part_rows, prompts, first, fill):
    base = jnp.full((prompts,) + part_rows.shape[1:], fill, jnp.float32)
    return lax.dynamic_update_slice_in_dim(base, part_rows, first, 0)


def cache_read(query_new, key_new, value_new, keys, values, mix_lambda, head_gain, first):
    count, span = (keys.shape[0], keys.shape[1])
    prompts = query_new.shape[0]
    heads = mix_lambda.shape[0]
    query = lax.dynamic_slice_in_dim(query_new, first, count, 0)
    scores = score_maps(query, keys)
    fresh_all = own_scores(query_new, key_new)
    fresh = lax.dynamic_slice_in_dim(fresh_all, first, count, 0)
    local_top = jnp.maximum(jnp.max(scores, axis=-1), fresh)
    local_total = jnp.sum(jnp.exp(scores - local_top[..., None]), axis=-1)
    top_all, cache_total = combined_all(
        (placed(local_top, prompts, first, -1e30), placed(local_total, prompts, first, 0.0)),
        "sp",
        join_totals,
    )
    own = jnp.exp(fresh_all - top_all)
    total_all = cache_total + own
    top = lax.dynamic_slice_in_dim(top_all, first, count, 0)
    total = lax.dynamic_slice_in_dim(total_all, first, count, 0)
    probs = jnp.exp(scores - top[..., None]) / total[..., None]
    mixed = (probs[:, :, 0] - mix_lambda[None, :, None] * probs[:, :, 1]).astype(jnp.bfloat16)
    value_parts = values.reshape(count, span, heads, VDIM)
    partial_value = jnp.einsum(
        "shl,slhv->shv", mixed, value_parts, preferred_element_type=jnp.float32
    )
    reads = lax.psum(placed(partial_value, prompts, first, 0.0), "sp")
    own_prob = own / total_all
    own_mixed = (own_prob[:, :, 0] - mix_lambda[None, :] * own_prob[:, :, 1]).astype(jnp.bfloat16)
    reads = reads + own_mixed.astype(jnp.float32)[..., None] * value_new.astype(
        jnp.float32
    ).reshape(prompts, heads, VDIM)
    return finish(reads, head_gain)


def block_read(
    query_new, key_new, value_new, key_cache, value_cache, mix_lambda, head_gain, spread
):
    blocks, sub = (key_cache.shape[1], key_cache.shape[2])
    first = lax.axis_index("sp") // spread
    keys = key_cache.reshape(1, blocks * sub, -1)
    values = value_cache.reshape(1, blocks * sub, -1)
    return cache_read(query_new, key_new, value_new, keys, values, mix_lambda, head_gain, first)


def body(prompt, w_key, w_value, query_new, key_new, value_new, mix_lambda, head_gain):
    count, piece, width = prompt.shape
    spread = lax.axis_size("sp") // count
    sub = piece // spread
    keys, values = project(prompt.reshape(count * piece, width), w_key, w_value)
    key_blocks = keys.reshape(count * spread, 1, sub, -1)
    value_blocks = values.reshape(count * spread, 1, sub, -1)
    key_cache, value_cache = (
        lax.all_to_all(key_blocks, "sp", split_axis=0, concat_axis=1, tiled=True),
        lax.all_to_all(value_blocks, "sp", split_axis=0, concat_axis=1, tiled=True),
    )
    first_read = block_read(
        query_new, key_new, value_new, key_cache, value_cache, mix_lambda, head_gain, spread
    )
    return (key_cache, value_cache, first_read)


def critical(n, spot):
    return n // 2 - 1 if spot >= n // 2 else n // 2


def crosses(n, src, dst):
    return critical(n, dst) == src


def right_plan(n, blocks, src):
    far_first = list(range(n - 1, src, -1))
    if src == n // 2 - 1:
        early = [(dst, "fill", 0) for dst in far_first]
        late = [(dst, "big", j) for j in range(blocks - 1) for dst in far_first]
        late += [(dst, "small", j) for j in range(2) for dst in far_first]
        return early, late
    if src < n // 2 - 1:
        near = [dst for dst in far_first if dst < n // 2]
        rest = [dst for dst in far_first if dst >= n // 2]
        return (
            [(dst, "big", j) for j in range(blocks) for dst in near],
            [(dst, "big", j) for j in range(blocks) for dst in rest],
        )
    early = [(dst, "big", 0) for dst in far_first]
    return early, [(dst, "big", j) for j in range(1, blocks) for dst in far_first]


def left_plan(n, blocks, src):
    early, late = right_plan(n, blocks, n - 1 - src)
    flip = lambda items: [(n - 1 - dst, kind, j) for dst, kind, j in items]
    return flip(early), flip(late)


def arrivals(n, blocks, spot):
    if spot >= n // 2:
        first, rest = arrivals(n, blocks, n - 1 - spot)
        flip = lambda items: [(kind, n - 1 - src, j) for kind, src, j in items]
        return flip(first), flip(rest)
    crit = n // 2
    same = sorted((s for s in range(n // 2) if s != spot), key=lambda s: abs(s - spot))
    other = [s for s in range(n // 2 + 1, n)]
    by_distance = sorted((s for s in range(n) if s != spot), key=lambda s: abs(s - spot))
    ahead = 3 if spot == n // 2 - 1 else 1
    near_w = [s for s in by_distance if abs(s - spot) == 1]
    far_w = [s for s in by_distance if abs(s - spot) > 1]
    first = [("w", s, 0) for s in near_w] + [("fill", crit, 0)]
    first += [("big", same[0], j) for j in range(ahead)]
    first += [("w", s, 0) for s in far_w]
    near = [("big", s, j) for j in range(blocks) for s in same][ahead:]
    through = [("big", s, j) for j in range(blocks) for s in other]
    last = [("big", crit, j) for j in range(blocks - 1)]
    if spot == n // 2 - 1:
        rest = near[:2] + last[:1] + near[2:] + through + last[1:]
    else:
        mixed = []
        for a in range(max(len(near), len(through))):
            mixed += near[a:a + 1] + through[a:a + 1]
        rest = last[:2] + mixed + last[2:]
    return first, rest


def gather_kernel(
    plan, prompt, w_key, w_value, query, key_new, value_new, lam, gain,
    keys, values, read,
    rows_in, weights, scores, q_low, own, slots,
    q_in, k_in, v_in, lam_in, gain_in,
    z_send, z_recv, x_send, x_recv, d_send, d_recv, e_send, e_recv,
    wr_send, wr_recv, wl_send, wl_recv, wy_send, wy_recv, s_send, s_recv, local,
):
    n, piece = plan
    blocks = piece // BIG
    slots_per = blocks + 2
    me = lax.axis_index("sp")
    tp = lax.axis_index("tp")
    grp = lax.axis_index("grp")
    across = lax.rem(tp + 2, 4)
    sibling = tp + 1 - 2 * lax.rem(tp, 2)
    far = lax.rem(sibling + 2, 4)
    depth, cols = w_key.shape
    heads = cols // VDIM
    half = depth // 2
    mats = (w_key, w_value)

    def by_spot(values_):
        pick = values_[0]
        for spot in range(1, n):
            pick = jnp.where(me == spot, values_[spot], pick)
        return pick

    crit = by_spot([critical(n, spot) for spot in range(n)])

    def span(kind, j):
        if kind == "big":
            return j * BIG, BIG, j
        if kind == "fill":
            return piece - BIG, FILL, blocks - 1
        return piece - 2 * SMALL + j * SMALL, SMALL, blocks + j

    def part(kind, j, q):
        start, size, _ = span(kind, j)
        quarter = size // 4
        return pl.ds(pl.multiple_of(start + q * quarter, quarter), quarter)

    barrier = pltpu.get_barrier_semaphore()
    for step in range(1, n):
        pl.semaphore_signal(
            barrier, inc=1, device_id={"sp": lax.rem(me + step, n)}, device_id_type=MESH
        )
    pl.semaphore_signal(barrier, inc=1, device_id={"tp": across}, device_id_type=MESH)
    pl.semaphore_signal(barrier, inc=1, device_id={"tp": sibling}, device_id_type=MESH)
    pl.semaphore_signal(barrier, inc=1, device_id={"grp": 1 - grp}, device_id_type=MESH)
    pl.semaphore_wait(barrier, n + 2)

    def w_slot(src, m, g):
        return weights.at[pl.ds(pl.multiple_of(src * depth + g * half, half), half),
                          pl.ds(m * cols, cols)]

    def w_hop(src, m, to, send, recv, own_):
        origin = mats[m].at[pl.ds(pl.multiple_of(grp * half, half), half)] if own_ else w_slot(src, m, grp)
        return pltpu.make_async_remote_copy(
            src_ref=origin, dst_ref=w_slot(src, m, grp),
            send_sem=send.at[src * 2 + m], recv_sem=recv.at[src * 2 + m],
            device_id={"sp": to}, device_id_type=MESH,
        )

    def w_side(src, m, g):
        return pltpu.make_async_remote_copy(
            src_ref=w_slot(src, m, g), dst_ref=w_slot(src, m, g),
            send_sem=wy_send.at[src * 2 + m], recv_sem=wy_recv.at[src * 2 + m],
            device_id={"grp": 1 - grp}, device_id_type=MESH,
        )

    def z_copy(src, dst, kind, j):
        at = span(kind, j)[2]
        return pltpu.make_async_remote_copy(
            src_ref=prompt.at[dst, part(kind, j, tp)], dst_ref=rows_in.at[src, part(kind, j, tp)],
            send_sem=z_send.at[dst * slots_per + at], recv_sem=z_recv.at[src * slots_per + at],
            device_id={"sp": dst}, device_id_type=MESH,
        )

    def side_copy(src, kind, j, q, to, send, recv):
        at = src * slots_per + span(kind, j)[2]
        return pltpu.make_async_remote_copy(
            src_ref=rows_in.at[src, part(kind, j, q)], dst_ref=rows_in.at[src, part(kind, j, q)],
            send_sem=send.at[at], recv_sem=recv.at[at],
            device_id={"tp": to}, device_id_type=MESH,
        )

    def take(src, kind, j):
        z_copy(src, me, kind, j).wait_recv()
        side_copy(src, kind, j, tp, across, x_send, x_recv).start()
        side_copy(src, kind, j, tp, sibling, d_send, d_recv).start()

    def relay(src, kind, j):
        side_copy(src, kind, j, across, across, x_send, x_recv).wait_recv()
        side_copy(src, kind, j, across, sibling, e_send, e_recv).start()

    def settle(src, kind, j):
        side_copy(src, kind, j, sibling, sibling, d_send, d_recv).wait_recv()
        side_copy(src, kind, j, far, sibling, e_send, e_recv).wait_recv()

    def send_all(items):
        for dst, kind, j in items:
            z_copy(me, dst, kind, j).start()

    for m in range(2):
        @pl.when(me + 1 < n)
        def _():
            w_hop(me, m, me + 1, wr_send, wr_recv, True).start()

        @pl.when(me > 0)
        def _():
            w_hop(me, m, me - 1, wl_send, wl_recv, True).start()

    for spot in range(n):
        @pl.when(me == spot)
        def _():
            send_all(right_plan(n, blocks, spot)[0])
            send_all(left_plan(n, blocks, spot)[0])

    small_in = [
        pltpu.make_async_copy(a, b, local.at[3 + i])
        for i, (a, b) in enumerate(
            ((query, q_in), (key_new, k_in), (value_new, v_in), (lam, lam_in), (gain, gain_in))
        )
    ]
    own_w = [
        pltpu.make_async_copy(
            mats[m],
            weights.at[pl.ds(pl.multiple_of(me * depth, depth), depth), pl.ds(m * cols, cols)],
            local.at[m],
        )
        for m in range(2)
    ]
    own_rows = pltpu.make_async_copy(prompt.at[me], rows_in.at[me], local.at[2])
    for copy in own_w + [own_rows] + small_in:
        copy.start()

    def weight_event(spot, src):
        for m in range(2):
            if src < spot:
                w_hop(src, m, me, wr_send, wr_recv, False).wait_recv()
                if spot + 1 < n:
                    w_hop(src, m, me + 1, wr_send, wr_recv, False).start()
            else:
                w_hop(src, m, me, wl_send, wl_recv, False).wait_recv()
                if spot > 0:
                    w_hop(src, m, me - 1, wl_send, wl_recv, False).start()
            w_side(src, m, grp).start()

    plans = [arrivals(n, blocks, spot) for spot in range(n)]
    aheads = [sum(kind == "big" for kind, _, _ in first) for first, _ in plans]
    orders = [
        [(s, j) for kind, s, j in first if kind == "big"] + [(s, j) for _, s, j in rest]
        for first, rest in plans
    ]
    total = len(orders[0])
    for spot in range(n):
        first = plans[spot][0]
        bigs = []

        @pl.when(me == spot)
        def _():
            lefts = [s for kind, s, _ in first if kind == "w" and s < spot]
            rights = [s for kind, s, _ in first if kind == "w" and s > spot]
            for kind, s, j in first:
                if kind == "w":
                    weight_event(spot, s)
                    if s < spot:
                        lefts.remove(s)
                        if not lefts:
                            send_all(right_plan(n, blocks, spot)[1])
                    else:
                        rights.remove(s)
                        if not rights:
                            send_all(left_plan(n, blocks, spot)[1])
                    continue
                take(s, kind, j)
                if kind == "big":
                    bigs.append((s, j))
                    if len(bigs) > 1:
                        relay(bigs[-2][0], "big", bigs[-2][1])
            relay(critical(n, spot), "fill", 0)
            if spot == 0:
                send_all(right_plan(n, blocks, spot)[1])
            if spot == n - 1:
                send_all(left_plan(n, blocks, spot)[1])

    for copy in small_in:
        copy.wait()

    def mine(ref):
        whole = ref[...].astype(jnp.float32)
        here = lax.broadcasted_iota(jnp.int32, whole.shape, 0) == me
        return jnp.sum(jnp.where(here, whole, 0.0), axis=0, keepdims=True)

    scale = HALF ** (-0.5)
    shape = (2 * heads, cols)
    row = lax.broadcasted_iota(jnp.int32, shape, 0)
    group = lax.broadcasted_iota(jnp.int32, shape, 1) // HALF
    chosen = jnp.where(row < heads, 2 * row, 2 * (row - heads) + 1) == group
    q_mat = jnp.where(chosen, jnp.broadcast_to(mine(q_in), shape), 0.0)
    fresh = jnp.sum(q_mat * mine(k_in), axis=1, keepdims=True) * scale
    q_low[...] = q_mat.astype(jnp.bfloat16)
    spread = (heads, heads)
    mix = jnp.sum(
        jnp.where(
            lax.broadcasted_iota(jnp.int32, spread, 0) == lax.broadcasted_iota(jnp.int32, spread, 1),
            jnp.broadcast_to(lam_in[...], spread), 0.0,
        ),
        axis=1, keepdims=True,
    )

    def project_rows(src, start, size):
        both = jnp.dot(
            rows_in[src, pl.ds(start, size), :], weights[...], preferred_element_type=jnp.float32
        ).astype(jnp.bfloat16)
        at = pl.ds(pl.multiple_of(src * piece + start, SMALL), size)
        keys[at, :] = both[:, :cols]
        values[at, :] = both[:, cols:]

    def score_rows(src, start, size):
        at = pl.multiple_of(src * piece + start, FILL)
        scores[:, pl.ds(at, size)] = lax.dot_general(
            q_low[...], keys[pl.ds(at, size), :], (((1,), (1,)), ((), ())),
            preferred_element_type=jnp.float32,
        ) * scale

    def compute(src, j):
        start = pl.multiple_of(j * BIG, BIG)
        project_rows(src, start, BIG)
        score_rows(src, start, BIG)

    picks = [by_spot([o[at][0] * blocks + o[at][1] for o in orders]) for at in range(total)]

    def order(k):
        pick = picks[0]
        for at in range(1, total):
            pick = jnp.where(k == at, picks[at], pick)
        return pick // blocks, lax.rem(pick, blocks)

    ahead = by_spot(aheads)

    def step(k, carry):
        @pl.when(k < total)
        def _():
            src, j = order(k)
            take_big(src, j)

        @pl.when(k - 1 < total)
        def _():
            src, j = order(k - 1)
            relay_big(src, j)

        @pl.when(k == ahead)
        def _():
            for step_ in range(1, n):
                src = lax.rem(me + step_, n)
                for m in range(2):
                    w_side(src, m, 1 - grp).wait_recv()
            for copy in own_w:
                copy.wait()
            own_rows.wait()

        @pl.when(k - ahead < blocks + ahead)
        def _():
            b = k - ahead
            src, j = order(b - blocks)
            foreign = b >= blocks

            @pl.when(foreign)
            def _():
                settle_big(src, j)

            compute(jnp.where(foreign, src, me), jnp.where(foreign, j, b))

        @pl.when(k - 2 >= ahead)
        def _():
            src, j = order(k - 2)
            settle_big(src, j)
            compute(src, j)

        return carry

    def dyn(j, q):
        quarter = BIG // 4
        return pl.ds(pl.multiple_of(j * BIG + q * quarter, quarter), quarter)

    def z_big(src, dst, j):
        return pltpu.make_async_remote_copy(
            src_ref=prompt.at[dst, dyn(j, tp)], dst_ref=rows_in.at[src, dyn(j, tp)],
            send_sem=z_send.at[dst * slots_per + j], recv_sem=z_recv.at[src * slots_per + j],
            device_id={"sp": dst}, device_id_type=MESH,
        )

    def side_big(src, j, q, to, send, recv):
        at = src * slots_per + j
        return pltpu.make_async_remote_copy(
            src_ref=rows_in.at[src, dyn(j, q)], dst_ref=rows_in.at[src, dyn(j, q)],
            send_sem=send.at[at], recv_sem=recv.at[at],
            device_id={"tp": to}, device_id_type=MESH,
        )

    def take_big(src, j):
        z_big(src, me, j).wait_recv()
        side_big(src, j, tp, across, x_send, x_recv).start()
        side_big(src, j, tp, sibling, d_send, d_recv).start()

    def relay_big(src, j):
        side_big(src, j, across, across, x_send, x_recv).wait_recv()
        side_big(src, j, across, sibling, e_send, e_recv).start()

    def settle_big(src, j):
        side_big(src, j, sibling, sibling, d_send, d_recv).wait_recv()
        side_big(src, j, far, sibling, e_send, e_recv).wait_recv()

    lax.fori_loop(ahead, total + 2, step, 0)

    last = piece - 2 * SMALL
    take(crit, "small", 0)
    settle(crit, "fill", 0)
    take(crit, "small", 1)
    relay(crit, "small", 0)
    settle(crit, "small", 0)
    project_rows(crit, piece - BIG, FILL + SMALL)
    score_rows(crit, piece - BIG, FILL)
    relay(crit, "small", 1)
    settle(crit, "small", 1)
    project_rows(crit, piece - SMALL, SMALL)
    score_rows(crit, last, 2 * SMALL)

    s = scores[...]
    top = jnp.maximum(jnp.max(s, axis=1, keepdims=True), fresh)
    e = jnp.exp(s - top)
    fresh_e = jnp.exp(fresh - top)
    sums = jnp.sum(e, axis=1, keepdims=True) + fresh_e
    w = e / sums
    fresh_w = fresh_e / sums
    mixed = (w[:heads] - mix * w[heads:]).astype(jnp.bfloat16)
    fresh_mixed = (fresh_w[:heads] - mix * fresh_w[heads:]).astype(jnp.bfloat16).astype(jnp.float32)
    o = jnp.dot(mixed, values[...], preferred_element_type=jnp.float32)
    o = o + fresh_mixed * mine(v_in)
    for h in range(heads):
        lanes = slice(h * VDIM, (h + 1) * VDIM)
        one = o[h:h + 1, lanes]
        mean = jnp.mean(one * one, axis=1, keepdims=True)
        own[:, lanes] = one * lax.rsqrt(mean + 1e-06) * gain_in[...]

    def row_copy(step_, src):
        return pltpu.make_async_remote_copy(
            src_ref=own, dst_ref=slots.at[src],
            send_sem=s_send.at[step_], recv_sem=s_recv.at[src],
            device_id={"sp": lax.rem(me + step_, n)}, device_id_type=MESH,
        )

    for step_ in range(1, n):
        row_copy(step_, me).start()

    for spot in range(n):
        @pl.when(me == spot)
        def _():
            for plan_ in (right_plan, left_plan):
                for dst, kind, j in sum(plan_(n, blocks, spot), []):
                    z_copy(me, dst, kind, j).wait_send()

    def drain(src, kind, j):
        side_copy(src, kind, j, tp, across, x_send, x_recv).wait_send()
        side_copy(src, kind, j, tp, sibling, d_send, d_recv).wait_send()
        side_copy(src, kind, j, across, sibling, e_send, e_recv).wait_send()

    def drain_big(k, carry):
        src, j = order(k)
        side_big(src, j, tp, across, x_send, x_recv).wait_send()
        side_big(src, j, tp, sibling, d_send, d_recv).wait_send()
        side_big(src, j, across, sibling, e_send, e_recv).wait_send()
        return carry

    lax.fori_loop(0, total, drain_big, 0)
    drain(crit, "fill", 0)
    drain(crit, "small", 0)
    drain(crit, "small", 1)
    for step_ in range(1, n):
        src = lax.rem(me + step_, n)
        for m in range(2):
            w_side(src, m, grp).wait_send()
    for d in range(n):
        for m in range(2):
            @pl.when((me - d >= 0) & (me + 1 < n))
            def _():
                w_hop(me - d, m, me + 1, wr_send, wr_recv, False).wait_send()

            @pl.when((me + d < n) & (me > 0))
            def _():
                w_hop(me + d, m, me - 1, wl_send, wl_recv, False).wait_send()

    for step_ in range(1, n):
        row_copy(step_, lax.rem(me + step_, n)).wait_recv()
    mine_row = own[...]
    for src in range(n):
        read[src:src + 1, :] = jnp.where(me == src, mine_row, slots[src]).astype(jnp.bfloat16)
    for step_ in range(1, n):
        row_copy(step_, me).wait_send()


def gather_project(n, prompt, w_key, w_value, query, key_new, value_new, mix_lambda, head_gain):
    count, piece, width = prompt.shape
    depth, cols = w_key.shape
    heads = mix_lambda.shape[0]
    dma = pltpu.SemaphoreType.DMA
    steps = n * (piece // BIG + 2)
    out = pltpu.VMEM((n * piece, cols), jnp.bfloat16)
    vmem = pl.BlockSpec(memory_space=pltpu.VMEM)
    hbm = pl.BlockSpec(memory_space=pltpu.HBM)
    f32, bf16 = jnp.float32, jnp.bfloat16
    return pl.pallas_call(
        functools.partial(gather_kernel, (n, piece)),
        out_shape=(out, out, pltpu.VMEM((n, cols), bf16)),
        in_specs=[hbm] * 8,
        out_specs=(vmem, vmem, vmem),
        scratch_shapes=[
            pltpu.VMEM((n, piece, width), bf16),
            pltpu.VMEM((n * depth, 2 * cols), bf16),
            pltpu.VMEM((2 * heads, n * piece), f32),
            pltpu.VMEM((2 * heads, cols), bf16),
            pltpu.VMEM((1, cols), f32),
            pltpu.VMEM((n, 1, cols), f32),
            pltpu.VMEM(query.shape, bf16),
            pltpu.VMEM(key_new.shape, bf16),
            pltpu.VMEM(value_new.shape, bf16),
            pltpu.VMEM((1, heads), f32),
            pltpu.VMEM((1, VDIM), f32),
        ]
        + [dma((steps,))] * 8
        + [dma((2 * n,))] * 6
        + [dma((n,))] * 2
        + [dma((8,))],
        compiler_params=pltpu.CompilerParams(
            collective_id=0, has_side_effects=True,
            vmem_limit_bytes=2**26 - 2**18 - 4 * n * piece * cols,
        ),
    )(
        prompt, w_key, w_value, query, key_new, value_new,
        mix_lambda[None, :], head_gain[None, :],
    )


def write_kernel(cuts, *refs):
    ins, outs, sem = refs[:3], refs[3:6], refs[6]
    copies = []
    for i in range(2):
        size = ins[i].shape[0] // cuts
        for c in range(cuts):
            at = pl.ds(c * size, size)
            copies.append((ins[i].at[at], outs[i].at[at]))
    copies.append((ins[2], outs[2]))
    copies = [pltpu.make_async_copy(a, b, sem.at[i]) for i, (a, b) in enumerate(copies)]
    for copy in copies:
        copy.start()
    for copy in copies:
        copy.wait()


def write_out(keys, values, read):
    cuts = 4
    hbm = pl.BlockSpec(memory_space=pltpu.HBM)
    vmem = pl.BlockSpec(memory_space=pltpu.VMEM)
    return pl.pallas_call(
        functools.partial(write_kernel, cuts),
        out_shape=tuple(jax.ShapeDtypeStruct(a.shape, a.dtype) for a in (keys, values, read)),
        in_specs=[vmem] * 3,
        out_specs=(hbm, hbm, hbm),
        scratch_shapes=[pltpu.SemaphoreType.DMA((2 * cuts + 1,))],
        compiler_params=pltpu.CompilerParams(vmem_limit_bytes=2**20),
    )(keys, values, read)


def fast_body(prompt, w_key, w_value, query_new, key_new, value_new, mix_lambda, head_gain):
    count, piece, width = prompt.shape
    n = lax.axis_size("sp")
    keys, values, read = write_out(
        *gather_project(
            n, prompt, w_key, w_value, query_new, key_new, value_new, mix_lambda, head_gain
        )
    )
    cols = keys.shape[-1]
    return (keys.reshape(1, n, piece, cols), values.reshape(1, n, piece, cols), read)


def choose(mesh):
    def run(prompt, *rest):
        sizes = dict(mesh.shape)
        count, piece, width = prompt.shape
        rows = rest[0].shape[0]
        fits = (
            sizes["grp"] == 2
            and sizes["tp"] == 4
            and sizes["sp"] == count
            and count % 2 == 0
            and count > 2
            and piece % BIG == 0
            and piece > 3 * BIG
            and rows % 32 == 0
            and count * piece * width * 2 <= 2**25
        )
        return (fast_body if fits else body)(prompt, *rest)

    return run


def solution(mesh):
    placed = (
        P("grp", "sp", None),
        P("sp", "tp"),
        P("sp", "tp"),
        P("grp", "tp"),
        P("grp", "tp"),
        P("grp", "tp"),
        P("tp"),
        P(),
    )
    return jax.shard_map(
        choose(mesh),
        mesh=mesh,
        in_specs=placed,
        out_specs=(
            P(("grp", "sp"), None, None, "tp"),
            P(("grp", "sp"), None, None, "tp"),
            P("grp", "tp"),
        ),
        check_vma=False,
    )
```

time: 192 us -> 188 us (0.979)
  local copies, waits for them, and re-layouts: 3.43 us -> 0 us
    unnamed x13 -> x0, local copies, waits for them, and re-layouts: 2.69 us -> none
    pallas_call x3 -> x2, Pallas kernels: 188 us -> 187 us  [the longest x1 182 us: gather_project(): pl.pallas_call(functools.partial(gather_kernel, (n, piece)), out_shape=(o...]
where the time goes in v1:
time: 188 us
  Pallas kernels  187 us (99%)
    pallas_call x1, Pallas kernels, gather_project(): pl.pallas_call(functools.partial(gather_kernel, (n, piece)), out_shape=(o...  182 us
    pallas_call x1, Pallas kernels, write_out(): pl.pallas_call(functools.partial(write_kernel, cuts), out_shape=tuple((ja...  4.67 us

profile of v1, /device:TPU:0, one launch (start us, length us, event | category | flops | bytes accessed | tf_op | source)
XLA Modules:
  0.0 187.6 jit_solution(10755893781699054751)
XLA Ops:
  0.6 182.3 %shard_map.103 = (bf16[6144,512]{1,0:T(8,128)(2,1)S(1)}, bf16[6144,512]{1,0:T(8,128)(2,1)S(1)}, bf16[4,512]{1,0:T(4,128)(2,1)S(1)}) custom-call(bf16[4,1536,2048]{2,1,0:T(8,128)(2,1)} %prompt.1, bf16[512,512]{1,0:T(8,128)(2,1)} %w_key.1, bf16[512,512]{1,0:T(8,128)(2,1)} %w_value.1, bf16[4,512]{1,0:T(4,128)(2,1)} %query.1, bf16[4,512]{1,0:T(4,128)(2,1)} %key_new.1, ...), custom_call_target="tpu_custom_call" | custom-call | tf_op jit(solution)/shard_map/pallas_call | solution.py:607
  182.9 4.7 %shard_map.104 = (bf16[6144,512]{1,0:T(8,128)(2,1)}, bf16[6144,512]{1,0:T(8,128)(2,1)}, bf16[4,512]{1,0:T(4,128)(2,1)}) custom-call(bf16[6144,512]{1,0:T(8,128)(2,1)S(1)} %get-tuple-element.9.refs_0_, bf16[6144,512]{1,0:T(8,128)(2,1)S(1)} %get-tuple-element.10.refs_1_, bf16[4,512]{1,0:T(4,128)(2,1)S(1)} %get-tuple-element.11.refs_2_), custom_call_target="tpu_custom_call" | custom-call | tf_op jit(solution)/shard_map/pallas_call | solution.py:659

commit v2 on v1

--- a/solution.py
+++ b/solution.py
@@ -11,8 +11,9 @@
 VDIM = 128
 MESH = pl.DeviceIdType.MESH
 BIG = 256
-FILL = 128
+MID = 128
 SMALL = 64
+START = 2
 
 
 def combined_all(part, axis, combine):
@@ -135,26 +136,28 @@
     return n // 2 - 1 if spot >= n // 2 else n // 2
 
 
-def crosses(n, src, dst):
-    return critical(n, dst) == src
+def tail_pieces(blocks):
+    return [("big", j) for j in range(blocks - 2)] + [
+        ("fill", 0), ("mid", 0), ("mid", 1), ("small", 0), ("small", 1)
+    ]
 
 
 def right_plan(n, blocks, src):
-    far_first = list(range(n - 1, src, -1))
-    if src == n // 2 - 1:
-        early = [(dst, "fill", 0) for dst in far_first]
-        late = [(dst, "big", j) for j in range(blocks - 1) for dst in far_first]
-        late += [(dst, "small", j) for j in range(2) for dst in far_first]
-        return early, late
-    if src < n // 2 - 1:
-        near = [dst for dst in far_first if dst < n // 2]
-        rest = [dst for dst in far_first if dst >= n // 2]
-        return (
-            [(dst, "big", j) for j in range(blocks) for dst in near],
-            [(dst, "big", j) for j in range(blocks) for dst in rest],
-        )
-    early = [(dst, "big", 0) for dst in far_first]
-    return early, [(dst, "big", j) for j in range(1, blocks) for dst in far_first]
+    far, near = n - 1, n // 2
+    every = [("big", j) for j in range(blocks)]
+    if src == 0:
+        return [(1, *p) for p in every], [(d, *p) for p in every for d in (far, near)]
+    if src == near:
+        return [(far, *p) for p in every[:1]], [(far, *p) for p in every[1:]]
+    if src == far:
+        return [], []
+    to_near = [(near, *p) for p in tail_pieces(blocks)]
+    to_far = [(far, *p) for p in tail_pieces(blocks)]
+    fill = blocks - 2
+    early = [to_near.pop(fill)]
+    late = to_near[:3] + to_far[:2] + to_near[3:4] + to_far[2:fill + 1]
+    rest = zip(to_far[fill + 1:], to_near[4:])
+    return early, late + [item for pair in rest for item in pair]
 
 
 def left_plan(n, blocks, src):
@@ -164,31 +167,22 @@
 
 
 def arrivals(n, blocks, spot):
-    if spot >= n // 2:
+    if spot < n // 2:
         first, rest = arrivals(n, blocks, n - 1 - spot)
         flip = lambda items: [(kind, n - 1 - src, j) for kind, src, j in items]
         return flip(first), flip(rest)
-    crit = n // 2
-    same = sorted((s for s in range(n // 2) if s != spot), key=lambda s: abs(s - spot))
-    other = [s for s in range(n // 2 + 1, n)]
-    by_distance = sorted((s for s in range(n) if s != spot), key=lambda s: abs(s - spot))
-    ahead = 3 if spot == n // 2 - 1 else 1
-    near_w = [s for s in by_distance if abs(s - spot) == 1]
-    far_w = [s for s in by_distance if abs(s - spot) > 1]
-    first = [("w", s, 0) for s in near_w] + [("fill", crit, 0)]
-    first += [("big", same[0], j) for j in range(ahead)]
-    first += [("w", s, 0) for s in far_w]
-    near = [("big", s, j) for j in range(blocks) for s in same][ahead:]
-    through = [("big", s, j) for j in range(blocks) for s in other]
-    last = [("big", crit, j) for j in range(blocks - 1)]
-    if spot == n // 2 - 1:
-        rest = near[:2] + last[:1] + near[2:] + through + last[1:]
-    else:
-        mixed = []
-        for a in range(max(len(near), len(through))):
-            mixed += near[a:a + 1] + through[a:a + 1]
-        rest = last[:2] + mixed + last[2:]
-    return first, rest
+    far = n - 1
+    crit = [("big", 1, j) for j in range(blocks - 2)]
+    through = [("big", 0, j) for j in range(blocks)]
+    if spot == far:
+        near = [("big", 2, j) for j in range(blocks)]
+        first = [("w", 2, 0), near[0], ("w", 1, 0), ("w", 0, 0)]
+        rest = [item for pair in zip(near[1:], through) for item in pair]
+        return first, rest + through[blocks - 1:] + crit
+    near = [("big", 3, j) for j in range(blocks)]
+    first = [("w", 1, 0), ("w", 3, 0), ("fill", 1, 0), near[0], near[1], ("w", 0, 0)]
+    rest = [near[2], crit[0], near[3], crit[1], near[4], crit[2], near[5]]
+    return first, rest + near[6:] + through + crit[3:]
 
 
 def gather_kernel(
@@ -196,12 +190,10 @@
     keys, values, read,
     rows_in, weights, scores, q_low, own, slots,
     q_in, k_in, v_in, lam_in, gain_in,
-    z_send, z_recv, x_send, x_recv, d_send, d_recv, e_send, e_recv,
-    wr_send, wr_recv, wl_send, wl_recv, wy_send, wy_recv, s_send, s_recv, local,
+    z_recv, x_recv, d_recv, w_recv, sent, met, local,
 ):
     n, piece = plan
     blocks = piece // BIG
-    slots_per = blocks + 2
     me = lax.axis_index("sp")
     tp = lax.axis_index("tp")
     grp = lax.axis_index("grp")
@@ -223,13 +215,20 @@
 
     def span(kind, j):
         if kind == "big":
-            return j * BIG, BIG, j
-        if kind == "fill":
-            return piece - BIG, FILL, blocks - 1
-        return piece - 2 * SMALL + j * SMALL, SMALL, blocks + j
+            return j * BIG, BIG
+        if kind == "small":
+            return piece - (2 - j) * SMALL, SMALL
+        return piece - 2 * BIG + (0 if kind == "fill" else 1 + j) * MID, MID
+
+    def flag(src, kind, j):
+        if kind == "small":
+            return n * blocks + 1 + j
+        if kind == "big":
+            return src * blocks + j
+        return n * blocks if (kind, j) == ("mid", 1) else src * blocks + blocks - 2 + (kind == "mid")
 
     def part(kind, j, q):
-        start, size, _ = span(kind, j)
+        start, size = span(kind, j)
         quarter = size // 4
         return pl.ds(pl.multiple_of(start + q * quarter, quarter), quarter)
 
@@ -247,49 +246,61 @@
         return weights.at[pl.ds(pl.multiple_of(src * depth + g * half, half), half),
                           pl.ds(m * cols, cols)]
 
-    def w_hop(src, m, to, send, recv, own_):
+    def w_hop(src, m, to, own_):
         origin = mats[m].at[pl.ds(pl.multiple_of(grp * half, half), half)] if own_ else w_slot(src, m, grp)
         return pltpu.make_async_remote_copy(
             src_ref=origin, dst_ref=w_slot(src, m, grp),
-            send_sem=send.at[src * 2 + m], recv_sem=recv.at[src * 2 + m],
+            send_sem=sent.at[0], recv_sem=w_recv.at[src * 2 + m],
             device_id={"sp": to}, device_id_type=MESH,
         )
 
     def w_side(src, m, g):
         return pltpu.make_async_remote_copy(
             src_ref=w_slot(src, m, g), dst_ref=w_slot(src, m, g),
-            send_sem=wy_send.at[src * 2 + m], recv_sem=wy_recv.at[src * 2 + m],
+            send_sem=sent.at[1], recv_sem=met.at[0],
             device_id={"grp": 1 - grp}, device_id_type=MESH,
         )
 
+    def w_all(count):
+        block = weights.at[pl.ds(0, count * half)]
+        return pltpu.make_async_remote_copy(
+            src_ref=block, dst_ref=block, send_sem=sent.at[1], recv_sem=met.at[0],
+            device_id={"grp": 1 - grp}, device_id_type=MESH,
+        )
+
     def z_copy(src, dst, kind, j):
-        at = span(kind, j)[2]
         return pltpu.make_async_remote_copy(
             src_ref=prompt.at[dst, part(kind, j, tp)], dst_ref=rows_in.at[src, part(kind, j, tp)],
-            send_sem=z_send.at[dst * slots_per + at], recv_sem=z_recv.at[src * slots_per + at],
+            send_sem=sent.at[2], recv_sem=z_recv.at[flag(src, kind, j)],
             device_id={"sp": dst}, device_id_type=MESH,
         )
 
     def side_copy(src, kind, j, q, to, send, recv):
-        at = src * slots_per + span(kind, j)[2]
         return pltpu.make_async_remote_copy(
             src_ref=rows_in.at[src, part(kind, j, q)], dst_ref=rows_in.at[src, part(kind, j, q)],
-            send_sem=send.at[at], recv_sem=recv.at[at],
+            send_sem=sent.at[send], recv_sem=recv.at[flag(src, kind, j)],
             device_id={"tp": to}, device_id_type=MESH,
+        )
+
+    def both_halves(src, start, size, at):
+        rows = rows_in.at[src, pl.ds(pl.multiple_of(start, size), size)]
+        return pltpu.make_async_remote_copy(
+            src_ref=rows, dst_ref=rows, send_sem=sent.at[4], recv_sem=d_recv.at[at],
+            device_id={"tp": sibling}, device_id_type=MESH,
         )
 
     def take(src, kind, j):
         z_copy(src, me, kind, j).wait_recv()
-        side_copy(src, kind, j, tp, across, x_send, x_recv).start()
-        side_copy(src, kind, j, tp, sibling, d_send, d_recv).start()
+        side_copy(src, kind, j, tp, across, 3, x_recv).start()
+        side_copy(src, kind, j, tp, sibling, 4, d_recv).start()
 
     def relay(src, kind, j):
-        side_copy(src, kind, j, across, across, x_send, x_recv).wait_recv()
-        side_copy(src, kind, j, across, sibling, e_send, e_recv).start()
+        side_copy(src, kind, j, across, across, 3, x_recv).wait_recv()
+        side_copy(src, kind, j, across, sibling, 5, d_recv).start()
 
     def settle(src, kind, j):
-        side_copy(src, kind, j, sibling, sibling, d_send, d_recv).wait_recv()
-        side_copy(src, kind, j, far, sibling, e_send, e_recv).wait_recv()
+        start, size = span(kind, j)
+        both_halves(src, start, size // 2, flag(src, kind, j)).wait_recv()
 
     def send_all(items):
         for dst, kind, j in items:
@@ -298,11 +309,11 @@
     for m in range(2):
         @pl.when(me + 1 < n)
         def _():
-            w_hop(me, m, me + 1, wr_send, wr_recv, True).start()
+            w_hop(me, m, me + 1, True).start()
 
         @pl.when(me > 0)
         def _():
-            w_hop(me, m, me - 1, wl_send, wl_recv, True).start()
+            w_hop(me, m, me - 1, True).start()
 
     for spot in range(n):
         @pl.when(me == spot)
@@ -331,13 +342,13 @@
     def weight_event(spot, src):
         for m in range(2):
             if src < spot:
-                w_hop(src, m, me, wr_send, wr_recv, False).wait_recv()
+                w_hop(src, m, me, False).wait_recv()
                 if spot + 1 < n:
-                    w_hop(src, m, me + 1, wr_send, wr_recv, False).start()
+                    w_hop(src, m, me + 1, False).start()
             else:
-                w_hop(src, m, me, wl_send, wl_recv, False).wait_recv()
+                w_hop(src, m, me, False).wait_recv()
                 if spot > 0:
-                    w_hop(src, m, me - 1, wl_send, wl_recv, False).start()
+                    w_hop(src, m, me - 1, False).start()
             w_side(src, m, grp).start()
 
     plans = [arrivals(n, blocks, spot) for spot in range(n)]
@@ -372,7 +383,8 @@
                     bigs.append((s, j))
                     if len(bigs) > 1:
                         relay(bigs[-2][0], "big", bigs[-2][1])
-            relay(critical(n, spot), "fill", 0)
+            if any(kind == "fill" for kind, _, _ in first):
+                relay(critical(n, spot), "fill", 0)
             if spot == 0:
                 send_all(right_plan(n, blocks, spot)[1])
             if spot == n - 1:
@@ -412,7 +424,7 @@
         values[at, :] = both[:, cols:]
 
     def score_rows(src, start, size):
-        at = pl.multiple_of(src * piece + start, FILL)
+        at = pl.multiple_of(src * piece + start, MID)
         scores[:, pl.ds(at, size)] = lax.dot_general(
             q_low[...], keys[pl.ds(at, size), :], (((1,), (1,)), ((), ())),
             preferred_element_type=jnp.float32,
@@ -434,29 +446,22 @@
     ahead = by_spot(aheads)
 
     def step(k, carry):
-        @pl.when(k < total)
-        def _():
-            src, j = order(k)
-            take_big(src, j)
-
-        @pl.when(k - 1 < total)
-        def _():
-            src, j = order(k - 1)
-            relay_big(src, j)
-
-        @pl.when(k == ahead)
-        def _():
-            for step_ in range(1, n):
-                src = lax.rem(me + step_, n)
-                for m in range(2):
-                    w_side(src, m, 1 - grp).wait_recv()
+        src, j = order(k)
+        take_big(src, j)
+        src, j = order(k - 1)
+        relay_big(src, j)
+
+        @pl.when(k == ahead + START)
+        def _():
+            w_all(n - 1).wait_recv()
             for copy in own_w:
                 copy.wait()
             own_rows.wait()
 
-        @pl.when(k - ahead < blocks + ahead)
-        def _():
-            b = k - ahead
+        b = k - ahead - START
+
+        @pl.when((b >= 0) & (b < blocks + ahead))
+        def _():
             src, j = order(b - blocks)
             foreign = b >= blocks
 
@@ -481,45 +486,80 @@
     def z_big(src, dst, j):
         return pltpu.make_async_remote_copy(
             src_ref=prompt.at[dst, dyn(j, tp)], dst_ref=rows_in.at[src, dyn(j, tp)],
-            send_sem=z_send.at[dst * slots_per + j], recv_sem=z_recv.at[src * slots_per + j],
+            send_sem=sent.at[2], recv_sem=z_recv.at[src * blocks + j],
             device_id={"sp": dst}, device_id_type=MESH,
         )
 
     def side_big(src, j, q, to, send, recv):
-        at = src * slots_per + j
         return pltpu.make_async_remote_copy(
             src_ref=rows_in.at[src, dyn(j, q)], dst_ref=rows_in.at[src, dyn(j, q)],
-            send_sem=send.at[at], recv_sem=recv.at[at],
+            send_sem=sent.at[send], recv_sem=recv.at[src * blocks + j],
             device_id={"tp": to}, device_id_type=MESH,
         )
 
     def take_big(src, j):
         z_big(src, me, j).wait_recv()
-        side_big(src, j, tp, across, x_send, x_recv).start()
-        side_big(src, j, tp, sibling, d_send, d_recv).start()
+        side_big(src, j, tp, across, 3, x_recv).start()
+        side_big(src, j, tp, sibling, 4, d_recv).start()
 
     def relay_big(src, j):
-        side_big(src, j, across, across, x_send, x_recv).wait_recv()
-        side_big(src, j, across, sibling, e_send, e_recv).start()
+        side_big(src, j, across, across, 3, x_recv).wait_recv()
+        side_big(src, j, across, sibling, 5, d_recv).start()
 
     def settle_big(src, j):
-        side_big(src, j, sibling, sibling, d_send, d_recv).wait_recv()
-        side_big(src, j, far, sibling, e_send, e_recv).wait_recv()
-
-    lax.fori_loop(ahead, total + 2, step, 0)
-
-    last = piece - 2 * SMALL
-    take(crit, "small", 0)
-    settle(crit, "fill", 0)
+        both_halves(src, j * BIG, BIG // 2, src * blocks + j).wait_recv()
+
+    lax.fori_loop(ahead, total, step, 0)
+
+    late_fill = (me == 0) | (me == n - 1)
+
+    @pl.when(late_fill)
+    def _():
+        take(crit, "fill", 0)
+
+    src, j = order(total - 1)
+    relay_big(src, j)
+
+    def last_bigs(k, carry):
+        src, j = order(k)
+
+        @pl.when(k < total)
+        def _():
+            settle_big(src, j)
+
+        @pl.when(k == total - 1)
+        def _():
+            take(crit, "mid", 0)
+
+            @pl.when(late_fill)
+            def _():
+                relay(crit, "fill", 0)
+
+        @pl.when(k == total)
+        def _():
+            take(crit, "mid", 1)
+            relay(crit, "mid", 0)
+            take(crit, "small", 0)
+            settle(crit, "fill", 0)
+            settle(crit, "mid", 0)
+
+        final = k == total
+        compute(jnp.where(final, crit, src), jnp.where(final, blocks - 2, j))
+        return carry
+
+    lax.fori_loop(total - 2, total + 1, last_bigs, 0)
+
     take(crit, "small", 1)
+    relay(crit, "mid", 1)
     relay(crit, "small", 0)
+    settle(crit, "mid", 1)
     settle(crit, "small", 0)
-    project_rows(crit, piece - BIG, FILL + SMALL)
-    score_rows(crit, piece - BIG, FILL)
+    project_rows(crit, piece - BIG, MID + SMALL)
+    score_rows(crit, piece - BIG, MID)
     relay(crit, "small", 1)
     settle(crit, "small", 1)
     project_rows(crit, piece - SMALL, SMALL)
-    score_rows(crit, last, 2 * SMALL)
+    score_rows(crit, piece - 2 * SMALL, 2 * SMALL)
 
     s = scores[...]
     top = jnp.maximum(jnp.max(s, axis=1, keepdims=True), fresh)
@@ -540,58 +580,41 @@
 
     def row_copy(step_, src):
         return pltpu.make_async_remote_copy(
-            src_ref=own, dst_ref=slots.at[src],
-            send_sem=s_send.at[step_], recv_sem=s_recv.at[src],
+            src_ref=own, dst_ref=slots.at[src], send_sem=sent.at[6], recv_sem=met.at[1],
             device_id={"sp": lax.rem(me + step_, n)}, device_id_type=MESH,
         )
 
     for step_ in range(1, n):
         row_copy(step_, me).start()
 
-    for spot in range(n):
-        @pl.when(me == spot)
-        def _():
-            for plan_ in (right_plan, left_plan):
-                for dst, kind, j in sum(plan_(n, blocks, spot), []):
-                    z_copy(me, dst, kind, j).wait_send()
-
-    def drain(src, kind, j):
-        side_copy(src, kind, j, tp, across, x_send, x_recv).wait_send()
-        side_copy(src, kind, j, tp, sibling, d_send, d_recv).wait_send()
-        side_copy(src, kind, j, across, sibling, e_send, e_recv).wait_send()
-
-    def drain_big(k, carry):
-        src, j = order(k)
-        side_big(src, j, tp, across, x_send, x_recv).wait_send()
-        side_big(src, j, tp, sibling, d_send, d_recv).wait_send()
-        side_big(src, j, across, sibling, e_send, e_recv).wait_send()
-        return carry
-
-    lax.fori_loop(0, total, drain_big, 0)
-    drain(crit, "fill", 0)
-    drain(crit, "small", 0)
-    drain(crit, "small", 1)
-    for step_ in range(1, n):
-        src = lax.rem(me + step_, n)
-        for m in range(2):
-            w_side(src, m, grp).wait_send()
-    for d in range(n):
-        for m in range(2):
-            @pl.when((me - d >= 0) & (me + 1 < n))
-            def _():
-                w_hop(me - d, m, me + 1, wr_send, wr_recv, False).wait_send()
-
-            @pl.when((me + d < n) & (me > 0))
-            def _():
-                w_hop(me + d, m, me - 1, wl_send, wl_recv, False).wait_send()
-
-    for step_ in range(1, n):
-        row_copy(step_, lax.rem(me + step_, n)).wait_recv()
+    def all_sent(block, at):
+        pltpu.make_async_remote_copy(
+            src_ref=block, dst_ref=block, send_sem=sent.at[at], recv_sem=met.at[1],
+            device_id={"sp": lax.rem(me + 1, n)}, device_id_type=MESH,
+        ).wait_send()
+
+    for at in range(2, 6):
+        all_sent(rows_in.at[0, pl.ds(0, (n - 1) * piece // 4)], at)
+    w_all(n - 1).wait_send()
+    inner = (me > 0) & (me + 1 < n)
+
+    @pl.when(inner)
+    def _():
+        all_sent(weights.at[pl.ds(0, (n + 1) * half)], 0)
+
+    @pl.when(jnp.logical_not(inner))
+    def _():
+        all_sent(weights.at[pl.ds(0, half)], 0)
+
+    others = slots.at[pl.ds(0, n - 1)]
+    pltpu.make_async_remote_copy(
+        src_ref=others, dst_ref=others, send_sem=sent.at[6], recv_sem=met.at[1],
+        device_id={"sp": lax.rem(me + 1, n)}, device_id_type=MESH,
+    ).wait_recv()
     mine_row = own[...]
     for src in range(n):
         read[src:src + 1, :] = jnp.where(me == src, mine_row, slots[src]).astype(jnp.bfloat16)
-    for step_ in range(1, n):
-        row_copy(step_, me).wait_send()
+    all_sent(others, 6)
 
 
 def gather_project(n, prompt, w_key, w_value, query, key_new, value_new, mix_lambda, head_gain):
@@ -599,7 +622,7 @@
     depth, cols = w_key.shape
     heads = mix_lambda.shape[0]
     dma = pltpu.SemaphoreType.DMA
-    steps = n * (piece // BIG + 2)
+    steps = n * (piece // BIG) + 3
     out = pltpu.VMEM((n * piece, cols), jnp.bfloat16)
     vmem = pl.BlockSpec(memory_space=pltpu.VMEM)
     hbm = pl.BlockSpec(memory_space=pltpu.HBM)
@@ -622,10 +645,8 @@
             pltpu.VMEM((1, heads), f32),
             pltpu.VMEM((1, VDIM), f32),
         ]
-        + [dma((steps,))] * 8
-        + [dma((2 * n,))] * 6
-        + [dma((n,))] * 2
-        + [dma((8,))],
+        + [dma((steps,))] * 3
+        + [dma((2 * n,)), dma((7,)), dma((2,)), dma((8,))],
         compiler_params=pltpu.CompilerParams(
             collective_id=0, has_side_effects=True,
             vmem_limit_bytes=2**26 - 2**18 - 4 * n * piece * cols,
@@ -687,10 +708,9 @@
             sizes["grp"] == 2
             and sizes["tp"] == 4
             and sizes["sp"] == count
-            and count % 2 == 0
-            and count > 2
+            and count == 4
             and piece % BIG == 0
-            and piece > 3 * BIG
+            and piece >= 6 * BIG
             and rows % 32 == 0
             and count * piece * width * 2 <= 2**25
         )

time: 188 us -> 181 us (0.963)
  Pallas kernels: 187 us -> 180 us
    pallas_call x1, Pallas kernels: 182 us -> 176 us  [gather_project(): pl.pallas_call(functools.partial(gather_kernel, (n, piece)), out_shape=(o...]
where the time goes in v2:
time: 181 us
  Pallas kernels  180 us (99%)
    pallas_call x1, Pallas kernels, gather_project(): pl.pallas_call(functools.partial(gather_kernel, (n, piece)), out_shape=(o...  176 us
    pallas_call x1, Pallas kernels, write_out(): pl.pallas_call(functools.partial(write_kernel, cuts), out_shape=tuple((ja...  4.67 us

profile of v2, /device:TPU:0, one launch (start us, length us, event | category | flops | bytes accessed | tf_op | source)
XLA Modules:
  0.0 181.0 jit_solution(5056661228196800415)
XLA Ops:
  0.6 175.6 %shard_map.103 = (bf16[6144,512]{1,0:T(8,128)(2,1)S(1)}, bf16[6144,512]{1,0:T(8,128)(2,1)S(1)}, bf16[4,512]{1,0:T(4,128)(2,1)S(1)}) custom-call(bf16[4,1536,2048]{2,1,0:T(8,128)(2,1)} %prompt.1, bf16[512,512]{1,0:T(8,128)(2,1)} %w_key.1, bf16[512,512]{1,0:T(8,128)(2,1)} %w_value.1, bf16[4,512]{1,0:T(4,128)(2,1)} %query.1, bf16[4,512]{1,0:T(4,128)(2,1)} %key_new.1, ...), custom_call_target="tpu_custom_call" | custom-call | tf_op jit(solution)/shard_map/pallas_call | solution.py:630
  176.3 4.7 %shard_map.104 = (bf16[6144,512]{1,0:T(8,128)(2,1)}, bf16[6144,512]{1,0:T(8,128)(2,1)}, bf16[4,512]{1,0:T(4,128)(2,1)}) custom-call(bf16[6144,512]{1,0:T(8,128)(2,1)S(1)} %get-tuple-element.9.refs_0_, bf16[6144,512]{1,0:T(8,128)(2,1)S(1)} %get-tuple-element.10.refs_1_, bf16[4,512]{1,0:T(4,128)(2,1)S(1)} %get-tuple-element.11.refs_2_), custom_call_target="tpu_custom_call" | custom-call | tf_op jit(solution)/shard_map/pallas_call | solution.py:680

commit v3 on v2

--- a/solution.py
+++ b/solution.py
@@ -11,9 +11,9 @@
 VDIM = 128
 MESH = pl.DeviceIdType.MESH
 BIG = 256
-MID = 128
-SMALL = 64
+TAIL = (128, 128, 128, 64, 32, 32)
 START = 2
+HOLD = 3
 
 
 def combined_all(part, axis, combine):
@@ -137,9 +137,7 @@
 
 
 def tail_pieces(blocks):
-    return [("big", j) for j in range(blocks - 2)] + [
-        ("fill", 0), ("mid", 0), ("mid", 1), ("small", 0), ("small", 1)
-    ]
+    return [("big", j) for j in range(blocks - 2)] + [("tail", j) for j in range(len(TAIL))]
 
 
 def right_plan(n, blocks, src):
@@ -180,7 +178,7 @@
         rest = [item for pair in zip(near[1:], through) for item in pair]
         return first, rest + through[blocks - 1:] + crit
     near = [("big", 3, j) for j in range(blocks)]
-    first = [("w", 1, 0), ("w", 3, 0), ("fill", 1, 0), near[0], near[1], ("w", 0, 0)]
+    first = [("w", 1, 0), ("w", 3, 0), ("tail", 1, 0), near[0], near[1], ("w", 0, 0)]
     rest = [near[2], crit[0], near[3], crit[1], near[4], crit[2], near[5]]
     return first, rest + near[6:] + through + crit[3:]
 
@@ -216,16 +214,12 @@
     def span(kind, j):
         if kind == "big":
             return j * BIG, BIG
-        if kind == "small":
-            return piece - (2 - j) * SMALL, SMALL
-        return piece - 2 * BIG + (0 if kind == "fill" else 1 + j) * MID, MID
+        return piece - sum(TAIL[j:]), TAIL[j]
 
     def flag(src, kind, j):
-        if kind == "small":
-            return n * blocks + 1 + j
         if kind == "big":
             return src * blocks + j
-        return n * blocks if (kind, j) == ("mid", 1) else src * blocks + blocks - 2 + (kind == "mid")
+        return src * blocks + blocks - 2 + j if j < 2 else n * blocks + j - 2
 
     def part(kind, j, q):
         start, size = span(kind, j)
@@ -233,14 +227,19 @@
         return pl.ds(pl.multiple_of(start + q * quarter, quarter), quarter)
 
     barrier = pltpu.get_barrier_semaphore()
-    for step in range(1, n):
-        pl.semaphore_signal(
-            barrier, inc=1, device_id={"sp": lax.rem(me + step, n)}, device_id_type=MESH
-        )
+
+    @pl.when(me + 1 < n)
+    def _():
+        pl.semaphore_signal(barrier, inc=1, device_id={"sp": me + 1}, device_id_type=MESH)
+
+    @pl.when(me > 0)
+    def _():
+        pl.semaphore_signal(barrier, inc=1, device_id={"sp": me - 1}, device_id_type=MESH)
+
     pl.semaphore_signal(barrier, inc=1, device_id={"tp": across}, device_id_type=MESH)
     pl.semaphore_signal(barrier, inc=1, device_id={"tp": sibling}, device_id_type=MESH)
     pl.semaphore_signal(barrier, inc=1, device_id={"grp": 1 - grp}, device_id_type=MESH)
-    pl.semaphore_wait(barrier, n + 2)
+    pl.semaphore_wait(barrier, jnp.where((me > 0) & (me + 1 < n), 5, 4))
 
     def w_slot(src, m, g):
         return weights.at[pl.ds(pl.multiple_of(src * depth + g * half, half), half),
@@ -372,23 +371,23 @@
                     if s < spot:
                         lefts.remove(s)
                         if not lefts:
-                            send_all(right_plan(n, blocks, spot)[1])
+                            send_all(right_plan(n, blocks, spot)[1][:HOLD])
                     else:
                         rights.remove(s)
                         if not rights:
-                            send_all(left_plan(n, blocks, spot)[1])
+                            send_all(left_plan(n, blocks, spot)[1][:HOLD])
                     continue
                 take(s, kind, j)
                 if kind == "big":
                     bigs.append((s, j))
                     if len(bigs) > 1:
                         relay(bigs[-2][0], "big", bigs[-2][1])
-            if any(kind == "fill" for kind, _, _ in first):
-                relay(critical(n, spot), "fill", 0)
-            if spot == 0:
-                send_all(right_plan(n, blocks, spot)[1])
-            if spot == n - 1:
-                send_all(left_plan(n, blocks, spot)[1])
+            if any(kind == "tail" for kind, _, _ in first):
+                relay(critical(n, spot), "tail", 0)
+            if spot > 0:
+                send_all(left_plan(n, blocks, spot)[1][HOLD if spot < n - 1 else 0:])
+            if spot < n - 1:
+                send_all(right_plan(n, blocks, spot)[1][HOLD if spot > 0 else 0:])
 
     for copy in small_in:
         copy.wait()
@@ -419,12 +418,12 @@
         both = jnp.dot(
             rows_in[src, pl.ds(start, size), :], weights[...], preferred_element_type=jnp.float32
         ).astype(jnp.bfloat16)
-        at = pl.ds(pl.multiple_of(src * piece + start, SMALL), size)
+        at = pl.ds(pl.multiple_of(src * piece + start, BIG), size)
         keys[at, :] = both[:, :cols]
         values[at, :] = both[:, cols:]
 
     def score_rows(src, start, size):
-        at = pl.multiple_of(src * piece + start, MID)
+        at = pl.multiple_of(src * piece + start, BIG)
         scores[:, pl.ds(at, size)] = lax.dot_general(
             q_low[...], keys[pl.ds(at, size), :], (((1,), (1,)), ((), ())),
             preferred_element_type=jnp.float32,
@@ -515,7 +514,7 @@
 
     @pl.when(late_fill)
     def _():
-        take(crit, "fill", 0)
+        take(crit, "tail", 0)
 
     src, j = order(total - 1)
     relay_big(src, j)
@@ -529,37 +528,35 @@
 
         @pl.when(k == total - 1)
         def _():
-            take(crit, "mid", 0)
+            take(crit, "tail", 1)
 
             @pl.when(late_fill)
             def _():
-                relay(crit, "fill", 0)
+                relay(crit, "tail", 0)
 
         @pl.when(k == total)
         def _():
-            take(crit, "mid", 1)
-            relay(crit, "mid", 0)
-            take(crit, "small", 0)
-            settle(crit, "fill", 0)
-            settle(crit, "mid", 0)
-
-        final = k == total
-        compute(jnp.where(final, crit, src), jnp.where(final, blocks - 2, j))
+            take(crit, "tail", 2)
+            relay(crit, "tail", 1)
+            take(crit, "tail", 3)
+            settle(crit, "tail", 0)
+            settle(crit, "tail", 1)
+
+        @pl.when(k == total + 1)
+        def _():
+            take(crit, "tail", 4)
+            relay(crit, "tail", 2)
+            take(crit, "tail", 5)
+            for piece_ in (3, 4, 5):
+                relay(crit, "tail", piece_)
+            for piece_ in (2, 3, 4, 5):
+                settle(crit, "tail", piece_)
+
+        final = k >= total
+        compute(jnp.where(final, crit, src), jnp.where(final, blocks - 2 + k - total, j))
         return carry
 
-    lax.fori_loop(total - 2, total + 1, last_bigs, 0)
-
-    take(crit, "small", 1)
-    relay(crit, "mid", 1)
-    relay(crit, "small", 0)
-    settle(crit, "mid", 1)
-    settle(crit, "small", 0)
-    project_rows(crit, piece - BIG, MID + SMALL)
-    score_rows(crit, piece - BIG, MID)
-    relay(crit, "small", 1)
-    settle(crit, "small", 1)
-    project_rows(crit, piece - SMALL, SMALL)
-    score_rows(crit, piece - 2 * SMALL, 2 * SMALL)
+    lax.fori_loop(total - 2, total + 2, last_bigs, 0)
 
     s = scores[...]
     top = jnp.maximum(jnp.max(s, axis=1, keepdims=True), fresh)
@@ -622,7 +619,7 @@
     depth, cols = w_key.shape
     heads = mix_lambda.shape[0]
     dma = pltpu.SemaphoreType.DMA
-    steps = n * (piece // BIG) + 3
+    steps = n * (piece // BIG) + len(TAIL) - 2
     out = pltpu.VMEM((n * piece, cols), jnp.bfloat16)
     vmem = pl.BlockSpec(memory_space=pltpu.VMEM)
     hbm = pl.BlockSpec(memory_space=pltpu.HBM)

time: 181 us -> 179 us (0.989)
  Pallas kernels: 180 us -> 178 us
    pallas_call x1, Pallas kernels: 176 us -> 173 us  [gather_project(): pl.pallas_call(functools.partial(gather_kernel, (n, piece)), out_shape=(o...]
where the time goes in v3:
time: 179 us
  Pallas kernels  178 us (99%)
    pallas_call x1, Pallas kernels, gather_project(): pl.pallas_call(functools.partial(gather_kernel, (n, piece)), out_shape=(o...  173 us
    pallas_call x1, Pallas kernels, write_out(): pl.pallas_call(functools.partial(write_kernel, cuts), out_shape=tuple((ja...  4.67 us

profile of v3, /device:TPU:0, one launch (start us, length us, event | category | flops | bytes accessed | tf_op | source)
XLA Modules:
  0.0 178.6 jit_solution(6477334957529147302)
XLA Ops:
  0.6 173.2 %shard_map.103 = (bf16[6144,512]{1,0:T(8,128)(2,1)S(1)}, bf16[6144,512]{1,0:T(8,128)(2,1)S(1)}, bf16[4,512]{1,0:T(4,128)(2,1)S(1)}) custom-call(bf16[4,1536,2048]{2,1,0:T(8,128)(2,1)} %prompt.1, bf16[512,512]{1,0:T(8,128)(2,1)} %w_key.1, bf16[512,512]{1,0:T(8,128)(2,1)} %w_value.1, bf16[4,512]{1,0:T(4,128)(2,1)} %query.1, bf16[4,512]{1,0:T(4,128)(2,1)} %key_new.1, ...), custom_call_target="tpu_custom_call" | custom-call | tf_op jit(solution)/shard_map/pallas_call | solution.py:627
  173.9 4.7 %shard_map.104 = (bf16[6144,512]{1,0:T(8,128)(2,1)}, bf16[6144,512]{1,0:T(8,128)(2,1)}, bf16[4,512]{1,0:T(4,128)(2,1)}) custom-call(bf16[6144,512]{1,0:T(8,128)(2,1)S(1)} %get-tuple-element.9.refs_0_, bf16[6144,512]{1,0:T(8,128)(2,1)S(1)} %get-tuple-element.10.refs_1_, bf16[4,512]{1,0:T(4,128)(2,1)S(1)} %get-tuple-element.11.refs_2_), custom_call_target="tpu_custom_call" | custom-call | tf_op jit(solution)/shard_map/pallas_call | solution.py:677

commit v4 on v3

--- a/solution.py
+++ b/solution.py
@@ -187,7 +187,7 @@
     plan, prompt, w_key, w_value, query, key_new, value_new, lam, gain,
     keys, values, read,
     rows_in, weights, scores, q_low, own, slots,
-    q_in, k_in, v_in, lam_in, gain_in,
+    new_in, lam_in, gain_in,
     z_recv, x_recv, d_recv, w_recv, sent, met, local,
 ):
     n, piece = plan
@@ -216,16 +216,25 @@
             return j * BIG, BIG
         return piece - sum(TAIL[j:]), TAIL[j]
 
-    def flag(src, kind, j):
+    def big_flag(src, dst, j):
+        return lax.rem(src - dst - 1 + n, n) * blocks + j
+
+    def flag(src, dst, kind, j):
         if kind == "big":
-            return src * blocks + j
-        return src * blocks + blocks - 2 + j if j < 2 else n * blocks + j - 2
+            return big_flag(src, dst, j)
+        return big_flag(src, dst, blocks - 2 + j) if j < 2 else (n - 1) * blocks + j - 2
 
     def part(kind, j, q):
         start, size = span(kind, j)
         quarter = size // 4
         return pl.ds(pl.multiple_of(start + q * quarter, quarter), quarter)
 
+    mine_w = pl.ds(pl.multiple_of(me * depth, depth), depth)
+    for m in range(2):
+        pltpu.make_async_copy(
+            mats[m], weights.at[mine_w, pl.ds(m * cols, cols)], local.at[0]
+        ).start()
+
     barrier = pltpu.get_barrier_semaphore()
 
     @pl.when(me + 1 < n)
@@ -240,15 +249,15 @@
     pl.semaphore_signal(barrier, inc=1, device_id={"tp": sibling}, device_id_type=MESH)
     pl.semaphore_signal(barrier, inc=1, device_id={"grp": 1 - grp}, device_id_type=MESH)
     pl.semaphore_wait(barrier, jnp.where((me > 0) & (me + 1 < n), 5, 4))
+    pltpu.make_async_copy(weights.at[mine_w], weights.at[mine_w], local.at[0]).wait()
 
     def w_slot(src, m, g):
         return weights.at[pl.ds(pl.multiple_of(src * depth + g * half, half), half),
                           pl.ds(m * cols, cols)]
 
-    def w_hop(src, m, to, own_):
-        origin = mats[m].at[pl.ds(pl.multiple_of(grp * half, half), half)] if own_ else w_slot(src, m, grp)
-        return pltpu.make_async_remote_copy(
-            src_ref=origin, dst_ref=w_slot(src, m, grp),
+    def w_hop(src, m, to):
+        return pltpu.make_async_remote_copy(
+            src_ref=w_slot(src, m, grp), dst_ref=w_slot(src, m, grp),
             send_sem=sent.at[0], recv_sem=w_recv.at[src * 2 + m],
             device_id={"sp": to}, device_id_type=MESH,
         )
@@ -256,7 +265,7 @@
     def w_side(src, m, g):
         return pltpu.make_async_remote_copy(
             src_ref=w_slot(src, m, g), dst_ref=w_slot(src, m, g),
-            send_sem=sent.at[1], recv_sem=met.at[0],
+            send_sem=sent.at[0], recv_sem=met.at[0],
             device_id={"grp": 1 - grp}, device_id_type=MESH,
         )
 
@@ -270,36 +279,49 @@
     def z_copy(src, dst, kind, j):
         return pltpu.make_async_remote_copy(
             src_ref=prompt.at[dst, part(kind, j, tp)], dst_ref=rows_in.at[src, part(kind, j, tp)],
-            send_sem=sent.at[2], recv_sem=z_recv.at[flag(src, kind, j)],
+            send_sem=sent.at[1], recv_sem=z_recv.at[flag(src, dst, kind, j)],
             device_id={"sp": dst}, device_id_type=MESH,
         )
 
-    def side_copy(src, kind, j, q, to, send, recv):
+    def side_copy(src, kind, j, q, to, recv):
         return pltpu.make_async_remote_copy(
             src_ref=rows_in.at[src, part(kind, j, q)], dst_ref=rows_in.at[src, part(kind, j, q)],
-            send_sem=sent.at[send], recv_sem=recv.at[flag(src, kind, j)],
+            send_sem=sent.at[1], recv_sem=recv.at[flag(src, me, kind, j)],
             device_id={"tp": to}, device_id_type=MESH,
         )
 
     def both_halves(src, start, size, at):
         rows = rows_in.at[src, pl.ds(pl.multiple_of(start, size), size)]
         return pltpu.make_async_remote_copy(
-            src_ref=rows, dst_ref=rows, send_sem=sent.at[4], recv_sem=d_recv.at[at],
+            src_ref=rows, dst_ref=rows, send_sem=sent.at[1], recv_sem=d_recv.at[at],
             device_id={"tp": sibling}, device_id_type=MESH,
         )
+
+    even = lax.rem(tp, 2) == 0
+
+    def skips(kind, j):
+        return kind == "tail" and j >= len(TAIL) - 2
 
     def take(src, kind, j):
         z_copy(src, me, kind, j).wait_recv()
-        side_copy(src, kind, j, tp, across, 3, x_recv).start()
-        side_copy(src, kind, j, tp, sibling, 4, d_recv).start()
+        side_copy(src, kind, j, tp, across, x_recv).start()
+        if skips(kind, j):
+            @pl.when(even)
+            def _():
+                side_copy(src, kind, j, tp, far, d_recv).start()
+
+        side_copy(src, kind, j, tp, sibling, d_recv).start()
 
     def relay(src, kind, j):
-        side_copy(src, kind, j, across, across, 3, x_recv).wait_recv()
-        side_copy(src, kind, j, across, sibling, 5, d_recv).start()
+        side_copy(src, kind, j, across, across, x_recv).wait_recv()
+
+        @pl.when(jnp.logical_not(even & skips(kind, j)))
+        def _():
+            side_copy(src, kind, j, across, sibling, d_recv).start()
 
     def settle(src, kind, j):
         start, size = span(kind, j)
-        both_halves(src, start, size // 2, flag(src, kind, j)).wait_recv()
+        both_halves(src, start, size // 2, flag(src, me, kind, j)).wait_recv()
 
     def send_all(items):
         for dst, kind, j in items:
@@ -308,11 +330,11 @@
     for m in range(2):
         @pl.when(me + 1 < n)
         def _():
-            w_hop(me, m, me + 1, True).start()
+            w_hop(me, m, me + 1).start()
 
         @pl.when(me > 0)
         def _():
-            w_hop(me, m, me - 1, True).start()
+            w_hop(me, m, me - 1).start()
 
     for spot in range(n):
         @pl.when(me == spot)
@@ -320,34 +342,27 @@
             send_all(right_plan(n, blocks, spot)[0])
             send_all(left_plan(n, blocks, spot)[0])
 
+    own_rows = pltpu.make_async_copy(prompt.at[me], rows_in.at[me], local.at[1])
     small_in = [
-        pltpu.make_async_copy(a, b, local.at[3 + i])
-        for i, (a, b) in enumerate(
-            ((query, q_in), (key_new, k_in), (value_new, v_in), (lam, lam_in), (gain, gain_in))
+        pltpu.make_async_copy(a, b, local.at[at])
+        for a, b, at in (
+            (query, new_in.at[0], 2), (key_new, new_in.at[1], 2), (value_new, new_in.at[2], 2),
+            (lam, lam_in, 3), (gain, gain_in, 4),
         )
     ]
-    own_w = [
-        pltpu.make_async_copy(
-            mats[m],
-            weights.at[pl.ds(pl.multiple_of(me * depth, depth), depth), pl.ds(m * cols, cols)],
-            local.at[m],
-        )
-        for m in range(2)
-    ]
-    own_rows = pltpu.make_async_copy(prompt.at[me], rows_in.at[me], local.at[2])
-    for copy in own_w + [own_rows] + small_in:
+    for copy in [own_rows] + small_in:
         copy.start()
 
     def weight_event(spot, src):
         for m in range(2):
             if src < spot:
-                w_hop(src, m, me, False).wait_recv()
+                w_hop(src, m, me).wait_recv()
                 if spot + 1 < n:
-                    w_hop(src, m, me + 1, False).start()
+                    w_hop(src, m, me + 1).start()
             else:
-                w_hop(src, m, me, False).wait_recv()
+                w_hop(src, m, me).wait_recv()
                 if spot > 0:
-                    w_hop(src, m, me - 1, False).start()
+                    w_hop(src, m, me - 1).start()
             w_side(src, m, grp).start()
 
     plans = [arrivals(n, blocks, spot) for spot in range(n)]
@@ -389,11 +404,12 @@
             if spot < n - 1:
                 send_all(right_plan(n, blocks, spot)[1][HOLD if spot > 0 else 0:])
 
-    for copy in small_in:
+    pltpu.make_async_copy(new_in, new_in, local.at[2]).wait()
+    for copy in small_in[3:]:
         copy.wait()
 
-    def mine(ref):
-        whole = ref[...].astype(jnp.float32)
+    def mine(which):
+        whole = new_in[which].astype(jnp.float32)
         here = lax.broadcasted_iota(jnp.int32, whole.shape, 0) == me
         return jnp.sum(jnp.where(here, whole, 0.0), axis=0, keepdims=True)
 
@@ -402,8 +418,8 @@
     row = lax.broadcasted_iota(jnp.int32, shape, 0)
     group = lax.broadcasted_iota(jnp.int32, shape, 1) // HALF
     chosen = jnp.where(row < heads, 2 * row, 2 * (row - heads) + 1) == group
-    q_mat = jnp.where(chosen, jnp.broadcast_to(mine(q_in), shape), 0.0)
-    fresh = jnp.sum(q_mat * mine(k_in), axis=1, keepdims=True) * scale
+    q_mat = jnp.where(chosen, jnp.broadcast_to(mine(0), shape), 0.0)
+    fresh = jnp.sum(q_mat * mine(1), axis=1, keepdims=True) * scale
     q_low[...] = q_mat.astype(jnp.bfloat16)
     spread = (heads, heads)
     mix = jnp.sum(
@@ -418,12 +434,12 @@
         both = jnp.dot(
             rows_in[src, pl.ds(start, size), :], weights[...], preferred_element_type=jnp.float32
         ).astype(jnp.bfloat16)
-        at = pl.ds(pl.multiple_of(src * piece + start, BIG), size)
+        at = pl.ds(pl.multiple_of(src * piece + start, BIG // 2), size)
         keys[at, :] = both[:, :cols]
         values[at, :] = both[:, cols:]
 
     def score_rows(src, start, size):
-        at = pl.multiple_of(src * piece + start, BIG)
+        at = pl.multiple_of(src * piece + start, BIG // 2)
         scores[:, pl.ds(at, size)] = lax.dot_general(
             q_low[...], keys[pl.ds(at, size), :], (((1,), (1,)), ((), ())),
             preferred_element_type=jnp.float32,
@@ -453,8 +469,6 @@
         @pl.when(k == ahead + START)
         def _():
             w_all(n - 1).wait_recv()
-            for copy in own_w:
-                copy.wait()
             own_rows.wait()
 
         b = k - ahead - START
@@ -485,28 +499,28 @@
     def z_big(src, dst, j):
         return pltpu.make_async_remote_copy(
             src_ref=prompt.at[dst, dyn(j, tp)], dst_ref=rows_in.at[src, dyn(j, tp)],
-            send_sem=sent.at[2], recv_sem=z_recv.at[src * blocks + j],
+            send_sem=sent.at[1], recv_sem=z_recv.at[big_flag(src, dst, j)],
             device_id={"sp": dst}, device_id_type=MESH,
         )
 
-    def side_big(src, j, q, to, send, recv):
+    def side_big(src, j, q, to, recv):
         return pltpu.make_async_remote_copy(
             src_ref=rows_in.at[src, dyn(j, q)], dst_ref=rows_in.at[src, dyn(j, q)],
-            send_sem=sent.at[send], recv_sem=recv.at[src * blocks + j],
+            send_sem=sent.at[1], recv_sem=recv.at[big_flag(src, me, j)],
             device_id={"tp": to}, device_id_type=MESH,
         )
 
     def take_big(src, j):
         z_big(src, me, j).wait_recv()
-        side_big(src, j, tp, across, 3, x_recv).start()
-        side_big(src, j, tp, sibling, 4, d_recv).start()
+        side_big(src, j, tp, across, x_recv).start()
+        side_big(src, j, tp, sibling, d_recv).start()
 
     def relay_big(src, j):
-        side_big(src, j, across, across, 3, x_recv).wait_recv()
-        side_big(src, j, across, sibling, 5, d_recv).start()
+        side_big(src, j, across, across, x_recv).wait_recv()
+        side_big(src, j, across, sibling, d_recv).start()
 
     def settle_big(src, j):
-        both_halves(src, j * BIG, BIG // 2, src * blocks + j).wait_recv()
+        both_halves(src, j * BIG, BIG // 2, big_flag(src, me, j)).wait_recv()
 
     lax.fori_loop(ahead, total, step, 0)
 
@@ -538,25 +552,40 @@
         def _():
             take(crit, "tail", 2)
             relay(crit, "tail", 1)
-            take(crit, "tail", 3)
+            for piece_ in (3, 4, 5):
+                take(crit, "tail", piece_)
+            relay(crit, "tail", 2)
             settle(crit, "tail", 0)
             settle(crit, "tail", 1)
 
-        @pl.when(k == total + 1)
-        def _():
-            take(crit, "tail", 4)
-            relay(crit, "tail", 2)
-            take(crit, "tail", 5)
+        final = k == total
+        compute(jnp.where(final, crit, src), jnp.where(final, blocks - 2, j))
+        return carry
+
+    lax.fori_loop(total - 2, total + 1, last_bigs, 0)
+
+    def last_rows(i, carry):
+        @pl.when(i == 0)
+        def _():
+            relay(crit, "tail", 3)
+            settle(crit, "tail", 2)
+
+        @pl.when((i == 0) != even)
+        def _():
+            for piece_ in (4, 5):
+                relay(crit, "tail", piece_)
+
+        @pl.when(i == 1)
+        def _():
             for piece_ in (3, 4, 5):
-                relay(crit, "tail", piece_)
-            for piece_ in (2, 3, 4, 5):
                 settle(crit, "tail", piece_)
 
-        final = k >= total
-        compute(jnp.where(final, crit, src), jnp.where(final, blocks - 2 + k - total, j))
+        start = pl.multiple_of(piece - BIG + i * (BIG // 2), BIG // 2)
+        project_rows(crit, start, BIG // 2)
+        score_rows(crit, start, BIG // 2)
         return carry
 
-    lax.fori_loop(total - 2, total + 2, last_bigs, 0)
+    lax.fori_loop(0, 2, last_rows, 0)
 
     s = scores[...]
     top = jnp.maximum(jnp.max(s, axis=1, keepdims=True), fresh)
@@ -568,7 +597,7 @@
     mixed = (w[:heads] - mix * w[heads:]).astype(jnp.bfloat16)
     fresh_mixed = (fresh_w[:heads] - mix * fresh_w[heads:]).astype(jnp.bfloat16).astype(jnp.float32)
     o = jnp.dot(mixed, values[...], preferred_element_type=jnp.float32)
-    o = o + fresh_mixed * mine(v_in)
+    o = o + fresh_mixed * mine(2)
     for h in range(heads):
         lanes = slice(h * VDIM, (h + 1) * VDIM)
         one = o[h:h + 1, lanes]
@@ -577,7 +606,7 @@
 
     def row_copy(step_, src):
         return pltpu.make_async_remote_copy(
-            src_ref=own, dst_ref=slots.at[src], send_sem=sent.at[6], recv_sem=met.at[1],
+            src_ref=own, dst_ref=slots.at[src], send_sem=sent.at[2], recv_sem=met.at[1],
             device_id={"sp": lax.rem(me + step_, n)}, device_id_type=MESH,
         )
 
@@ -590,28 +619,26 @@
             device_id={"sp": lax.rem(me + 1, n)}, device_id_type=MESH,
         ).wait_send()
 
-    for at in range(2, 6):
-        all_sent(rows_in.at[0, pl.ds(0, (n - 1) * piece // 4)], at)
-    w_all(n - 1).wait_send()
+    all_sent(rows_in.at[pl.ds(0, n - 1)], 1)
     inner = (me > 0) & (me + 1 < n)
 
     @pl.when(inner)
     def _():
-        all_sent(weights.at[pl.ds(0, (n + 1) * half)], 0)
+        all_sent(weights.at[pl.ds(0, 2 * n * half)], 0)
 
     @pl.when(jnp.logical_not(inner))
     def _():
-        all_sent(weights.at[pl.ds(0, half)], 0)
+        all_sent(weights.at[pl.ds(0, n * half)], 0)
 
     others = slots.at[pl.ds(0, n - 1)]
     pltpu.make_async_remote_copy(
-        src_ref=others, dst_ref=others, send_sem=sent.at[6], recv_sem=met.at[1],
+        src_ref=others, dst_ref=others, send_sem=sent.at[2], recv_sem=met.at[1],
         device_id={"sp": lax.rem(me + 1, n)}, device_id_type=MESH,
     ).wait_recv()
     mine_row = own[...]
     for src in range(n):
         read[src:src + 1, :] = jnp.where(me == src, mine_row, slots[src]).astype(jnp.bfloat16)
-    all_sent(others, 6)
+    all_sent(others, 2)
 
 
 def gather_project(n, prompt, w_key, w_value, query, key_new, value_new, mix_lambda, head_gain):
@@ -619,7 +646,7 @@
     depth, cols = w_key.shape
     heads = mix_lambda.shape[0]
     dma = pltpu.SemaphoreType.DMA
-    steps = n * (piece // BIG) + len(TAIL) - 2
+    steps = (n - 1) * (piece // BIG) + len(TAIL) - 2
     out = pltpu.VMEM((n * piece, cols), jnp.bfloat16)
     vmem = pl.BlockSpec(memory_space=pltpu.VMEM)
     hbm = pl.BlockSpec(memory_space=pltpu.HBM)
@@ -636,14 +663,12 @@
             pltpu.VMEM((2 * heads, cols), bf16),
             pltpu.VMEM((1, cols), f32),
             pltpu.VMEM((n, 1, cols), f32),
-            pltpu.VMEM(query.shape, bf16),
-            pltpu.VMEM(key_new.shape, bf16),
-            pltpu.VMEM(value_new.shape, bf16),
+            pltpu.VMEM((3, *query.shape), bf16),
             pltpu.VMEM((1, heads), f32),
             pltpu.VMEM((1, VDIM), f32),
         ]
         + [dma((steps,))] * 3
-        + [dma((2 * n,)), dma((7,)), dma((2,)), dma((8,))],
+        + [dma((2 * n,)), dma((3,)), dma((2,)), dma((5,))],
         compiler_params=pltpu.CompilerParams(
             collective_id=0, has_side_effects=True,
             vmem_limit_bytes=2**26 - 2**18 - 4 * n * piece * cols,

time: 179 us -> 178 us (level)
  no operation moved by 1% of the time
where the time goes in v4:
time: 178 us
  Pallas kernels  177 us (99%)
    pallas_call x1, Pallas kernels, gather_project(): pl.pallas_call(functools.partial(gather_kernel, (n, piece)), out_shape=(o...  172 us
    pallas_call x1, Pallas kernels, write_out(): pl.pallas_call(functools.partial(write_kernel, cuts), out_shape=tuple((ja...  4.67 us

profile of v4, /device:TPU:0, one launch (start us, length us, event | category | flops | bytes accessed | tf_op | source)
XLA Modules:
  0.0 177.6 jit_solution(13004249242144684758)
XLA Ops:
  0.6 172.3 %shard_map.103 = (bf16[6144,512]{1,0:T(8,128)(2,1)S(1)}, bf16[6144,512]{1,0:T(8,128)(2,1)S(1)}, bf16[4,512]{1,0:T(4,128)(2,1)S(1)}) custom-call(bf16[4,1536,2048]{2,1,0:T(8,128)(2,1)} %prompt.1, bf16[512,512]{1,0:T(8,128)(2,1)} %w_key.1, bf16[512,512]{1,0:T(8,128)(2,1)} %w_value.1, bf16[4,512]{1,0:T(4,128)(2,1)} %query.1, bf16[4,512]{1,0:T(4,128)(2,1)} %key_new.1, ...), custom_call_target="tpu_custom_call" | custom-call | tf_op jit(solution)/shard_map/pallas_call | solution.py:654
  172.9 4.7 %shard_map.104 = (bf16[6144,512]{1,0:T(8,128)(2,1)}, bf16[6144,512]{1,0:T(8,128)(2,1)}, bf16[4,512]{1,0:T(4,128)(2,1)}) custom-call(bf16[6144,512]{1,0:T(8,128)(2,1)S(1)} %get-tuple-element.9.refs_0_, bf16[6144,512]{1,0:T(8,128)(2,1)S(1)} %get-tuple-element.10.refs_1_, bf16[4,512]{1,0:T(4,128)(2,1)S(1)} %get-tuple-element.11.refs_2_), custom_call_target="tpu_custom_call" | custom-call | tf_op jit(solution)/shard_map/pallas_call | solution.py:702

commit v5 on v4

--- a/solution.py
+++ b/solution.py
@@ -564,28 +564,34 @@
 
     lax.fori_loop(total - 2, total + 1, last_bigs, 0)
 
-    def last_rows(i, carry):
-        @pl.when(i == 0)
-        def _():
-            relay(crit, "tail", 3)
-            settle(crit, "tail", 2)
-
-        @pl.when((i == 0) != even)
-        def _():
-            for piece_ in (4, 5):
-                relay(crit, "tail", piece_)
-
-        @pl.when(i == 1)
-        def _():
-            for piece_ in (3, 4, 5):
-                settle(crit, "tail", piece_)
-
-        start = pl.multiple_of(piece - BIG + i * (BIG // 2), BIG // 2)
-        project_rows(crit, start, BIG // 2)
-        score_rows(crit, start, BIG // 2)
-        return carry
-
-    lax.fori_loop(0, 2, last_rows, 0)
+    relay(crit, "tail", 3)
+    settle(crit, "tail", 2)
+
+    @pl.when(jnp.logical_not(even))
+    def _():
+        for piece_ in (4, 5):
+            relay(crit, "tail", piece_)
+
+    project_rows(crit, piece - BIG, BIG // 2)
+    score_rows(crit, piece - BIG, BIG // 2)
+
+    @pl.when(even)
+    def _():
+        for piece_ in (4, 5):
+            relay(crit, "tail", piece_)
+
+    for piece_ in (3, 4, 5):
+        settle(crit, "tail", piece_)
+    rest = BIG // 2
+    rest_rows = rows_in[crit, piece - rest:, :]
+    at_rest = pl.ds(pl.multiple_of(crit * piece + piece - rest, rest), rest)
+    keys[at_rest, :] = jnp.dot(
+        rest_rows, weights[:, :cols], preferred_element_type=jnp.float32
+    ).astype(jnp.bfloat16)
+    score_rows(crit, piece - rest, rest)
+    values[at_rest, :] = jnp.dot(
+        rest_rows, weights[:, cols:], preferred_element_type=jnp.float32
+    ).astype(jnp.bfloat16)
 
     s = scores[...]
     top = jnp.maximum(jnp.max(s, axis=1, keepdims=True), fresh)

time: 178 us -> 178 us (level)
  no operation moved by 1% of the time
where the time goes in v5:
time: 178 us; the launch traced here: 177 us
  Pallas kernels  177 us (99%)
    pallas_call x1, Pallas kernels, gather_project(): pl.pallas_call(functools.partial(gather_kernel, (n, piece)), out_shape=(o...  172 us
    pallas_call x1, Pallas kernels, write_out(): pl.pallas_call(functools.partial(write_kernel, cuts), out_shape=tuple((ja...  4.67 us

profile of v5, /device:TPU:0, one launch (start us, length us, event | category | flops | bytes accessed | tf_op | source)
XLA Modules:
  0.0 177.5 jit_solution(11594406697931320426)
XLA Ops:
  0.6 172.2 %shard_map.103 = (bf16[6144,512]{1,0:T(8,128)(2,1)S(1)}, bf16[6144,512]{1,0:T(8,128)(2,1)S(1)}, bf16[4,512]{1,0:T(4,128)(2,1)S(1)}) custom-call(bf16[4,1536,2048]{2,1,0:T(8,128)(2,1)} %prompt.1, bf16[512,512]{1,0:T(8,128)(2,1)} %w_key.1, bf16[512,512]{1,0:T(8,128)(2,1)} %w_value.1, bf16[4,512]{1,0:T(4,128)(2,1)} %query.1, bf16[4,512]{1,0:T(4,128)(2,1)} %key_new.1, ...), custom_call_target="tpu_custom_call" | custom-call | tf_op jit(solution)/shard_map/pallas_call | solution.py:660
  172.8 4.7 %shard_map.104 = (bf16[6144,512]{1,0:T(8,128)(2,1)}, bf16[6144,512]{1,0:T(8,128)(2,1)}, bf16[4,512]{1,0:T(4,128)(2,1)}) custom-call(bf16[6144,512]{1,0:T(8,128)(2,1)S(1)} %get-tuple-element.9.refs_0_, bf16[6144,512]{1,0:T(8,128)(2,1)S(1)} %get-tuple-element.10.refs_1_, bf16[4,512]{1,0:T(4,128)(2,1)S(1)} %get-tuple-element.11.refs_2_), custom_call_target="tpu_custom_call" | custom-call | tf_op jit(solution)/shard_map/pallas_call | solution.py:708
